TPU v7x, 512 devices: a whole 4x4x16 slice. The times are simulated.
512 devices in a mesh: kv: 128 (over z, x, core), tp: 4 (over y).
Axes of the slice: x: 4, y: 4, z: 16, core: 2. Of those that a mesh axis runs over, the one named last changes fastest.
Arguments:
- queries: bfloat16 [1024, 4, 8, 128], P('kv', None, 'tp'), may hold values from -6 to 6
- keys: bfloat16 [1024, 4, 8, 128], P('kv', None, 'tp'), may hold values from -6 to 6
- values: bfloat16 [1024, 4, 8, 256], P('kv', None, 'tp'), may hold values from -6 to 6
- in_gate: float32 [1024, 4, 8], P('kv', None, 'tp'), may hold values from -6 to 6
- forget_pre: float32 [1024, 4, 8], P('kv', None, 'tp'), may hold values from -1 to 5
- old_keys: bfloat16 [1024, 4, 8, 128], P('kv', None, 'tp'), may hold values from -6 to 6
- old_values: bfloat16 [1024, 4, 8, 256], P('kv', None, 'tp'), may hold values from -6 to 6
- old_in_gate: float32 [1024, 4, 8], P('kv', None, 'tp'), may hold values from -6 to 6
- old_forget: float32 [1024, 4, 8], P('kv', None, 'tp'), may hold values from -1 to 5
- accepted: int32 [1024], P('kv'), may hold values from 0 to 4
- state_mem: float32 [1024, 8, 128, 256], P('kv', 'tp'), may hold values from -4 to 4
- state_norm: float32 [1024, 8, 128], P('kv', 'tp'), may hold values from -6 to 6
- state_max: float32 [1024, 8], P('kv', 'tp'), may hold values from -4 to 4
- norm_gain: float32 [8, 256], P('tp'), may hold values from 0.1 to 1.9
- out_weight: bfloat16 [2048, 2048], P('tp', 'kv'), may hold values from -0.125 to 0.125
Outputs:
- mixed: bfloat16 [1024, 4, 2048], P('kv', 'tp')
- new_mem: float32 [1024, 8, 128, 256], P('kv', 'tp')
- new_norm: float32 [1024, 8, 128], P('kv', 'tp')
- new_max: float32 [1024, 8], P('kv', 'tp')
Inputs may be any that keep to these rules, and one draw needn't show every extreme that they name: How many of the last step's 4 proposals of a sequence were accepted.
All inputs are finite; a program needn't handle non-finite values.
Results may differ from a plain program's by a relative error of at most 0.0068.
Values may be sent and summed in bfloat16 or wider, within the bound.
No kernel may reach another device: no remote copies, remote signals or barrier semaphores. Data moves between devices by JAX's collectives and lax.ppermute only.
A program may use at most 64 MiB of HBM per device.

v0:
```python
import jax
import jax.numpy as jnp
from jax import lax
from jax.sharding import Mesh
from jax.sharding import PartitionSpec as P

KV = ("kv_0", "kv_1", "kv_2")


HIGH = lax.Precision.HIGHEST


def sent_to_all(shard, axis):
    size = lax.axis_size(axis)
    return lax.all_to_all(
        jnp.broadcast_to(shard[None], (size, *shard.shape)), axis, 0, 0, tiled=True
    )


def joined_along(pieces, dim):
    pieces = jnp.moveaxis(pieces, 0, dim)
    shape = pieces.shape
    return pieces.reshape(*shape[:dim], shape[dim] * shape[dim + 1], *shape[dim + 2 :])


def gather_axes(shard, axes, dim):
    far, near = axes
    pieces = sent_to_all(sent_to_all(shard, far), near)
    return joined_along(pieces.swapaxes(0, 1).reshape(-1, *shard.shape), dim)


def cut_along(shard, dim, size):
    shape = shard.shape
    pieces = shard.reshape(*shape[:dim], size, shape[dim] // size, *shape[dim + 1 :])
    return jnp.moveaxis(pieces, dim, 0)


def summed_on_arrival(shard, axis, dim):
    pieces = cut_along(shard, dim, lax.axis_size(axis))
    arrived = lax.all_to_all(pieces, axis, split_axis=0, concat_axis=0, tiled=True)
    return arrived.astype(jnp.float32).sum(axis=0)


def cell(queries, keys, values, in_gates, log_forget, memory, normal, stab):
    length = in_gates.shape[-1]
    causal = jnp.tril(jnp.ones((length, length), dtype=bool))
    cumul = jnp.cumsum(log_forget, axis=-1)
    logd = jnp.where(causal, cumul[:, :, None] - cumul[:, None, :] + in_gates[:, None, :], -jnp.inf)
    inter = cumul + stab[:, None]
    m_row = jnp.maximum(inter, jnp.max(logd, axis=-1))
    scores = jnp.einsum("hld,hsd->hls", queries, keys, precision=HIGH) * jnp.exp(
        logd - m_row[..., None]
    )
    w_inter = jnp.exp(inter - m_row)
    num = w_inter[..., None] * jnp.einsum(
        "hld,hde->hle", queries, memory, precision=HIGH
    ) + jnp.einsum("hls,hse->hle", scores, values, precision=HIGH)
    den = w_inter * jnp.einsum("hld,hd->hl", queries, normal, precision=HIGH) + jnp.sum(
        scores, axis=-1
    )
    hidden = num / jnp.maximum(jnp.abs(den), 1.0)[..., None]
    m_new = m_row[:, -1]
    g_state = jnp.exp(cumul[:, -1] + stab - m_new)
    g_tok = jnp.exp(cumul[:, -1:] - cumul + in_gates - m_new[:, None])
    mem_new = g_state[:, None, None] * memory + jnp.einsum(
        "hld,hle->hde", g_tok[..., None] * keys, values, precision=HIGH
    )
    norm_new = g_state[:, None] * normal + jnp.einsum("hl,hld->hd", g_tok, keys, precision=HIGH)
    return (hidden, mem_new, norm_new, m_new)


def one_sequence(
    queries,
    keys,
    values,
    in_gate,
    forget_pre,
    old_keys,
    old_values,
    old_in_gate,
    old_forget,
    accepted,
    memory,
    normal,
    stab,
    norm_gain,
):
    props = queries.shape[0]
    live = jnp.arange(props, dtype=jnp.int32) < accepted
    gates = jnp.concatenate([jnp.where(live[:, None], old_in_gate, -jnp.inf), in_gate], axis=0)
    forget = jnp.concatenate(
        [
            jnp.where(live[:, None], jax.nn.log_sigmoid(old_forget), 0.0),
            jax.nn.log_sigmoid(forget_pre),
        ],
        axis=0,
    )
    scale = queries.shape[-1] ** (-0.5)
    qrun = jnp.concatenate(
        [jnp.zeros(queries.shape, jnp.float32), queries.astype(jnp.float32) * scale], axis=0
    )
    krun = jnp.concatenate([old_keys, keys], axis=0).astype(jnp.float32)
    vrun = jnp.concatenate([old_values, values], axis=0).astype(jnp.float32)
    hidden, mem_new, norm_new, m_new = cell(
        jnp.swapaxes(qrun, 0, 1),
        jnp.swapaxes(krun, 0, 1),
        jnp.swapaxes(vrun, 0, 1),
        gates.T,
        forget.T,
        memory,
        normal,
        stab,
    )
    hidden = hidden[:, props:, :]
    mean = jnp.mean(hidden, -1, keepdims=True)
    var = jnp.mean(jnp.square(hidden - mean), -1, keepdims=True)
    normed = (hidden - mean) * lax.rsqrt(var + 1e-05) * norm_gain[:, None, :]
    flat = jnp.swapaxes(normed, 0, 1).reshape(props, -1).astype(jnp.bfloat16)
    return (flat, mem_new, norm_new, m_new)


def on_device(
    queries,
    keys,
    values,
    in_gate,
    forget_pre,
    old_keys,
    old_values,
    old_in_gate,
    old_forget,
    accepted,
    state_mem,
    state_norm,
    state_max,
    norm_gain,
    out_weight,
):
    mapped = jax.vmap(one_sequence, in_axes=(0, 0, 0, 0, 0, 0, 0, 0, 0, 0, 0, 0, 0, None))
    hidden, new_mem, new_norm, new_max = mapped(
        queries,
        keys,
        values,
        in_gate,
        forget_pre,
        old_keys,
        old_values,
        old_in_gate,
        old_forget,
        accepted,
        state_mem,
        state_norm,
        state_max,
        norm_gain,
    )
    terms = jnp.einsum(
        "spr,rc->spc",
        hidden,
        gather_axes(out_weight, (("kv_0", "kv_1"), "kv_2"), 1),
        preferred_element_type=jnp.float32,
    )
    mixed = summed_on_arrival(terms.astype(jnp.bfloat16), "tp", 1).astype(jnp.bfloat16)
    return (mixed, new_mem, new_norm, new_max)


def solution(mesh):
    finer = Mesh(mesh.devices.reshape(16, 4, 2, mesh.shape["tp"]), ("kv_0", "kv_1", "kv_2", "tp"))
    in_specs = (
        P(KV, None, "tp", None),
        P(KV, None, "tp", None),
        P(KV, None, "tp", None),
        P(KV, None, "tp"),
        P(KV, None, "tp"),
        P(KV, None, "tp", None),
        P(KV, None, "tp", None),
        P(KV, None, "tp"),
        P(KV, None, "tp"),
        P(KV),
        P(KV, "tp", None, None),
        P(KV, "tp", None),
        P(KV, "tp"),
        P("tp", None),
        P("tp", KV),
    )
    out_specs = (P(KV, "tp", None), P(KV, "tp", None, None), P(KV, "tp", None), P(KV, "tp"))
    return jax.shard_map(
        on_device, mesh=finer, in_specs=in_specs, out_specs=out_specs, check_vma=False
    )
```

profile of v0, /device:TPU:2, one launch (start us, length us, event | category | flops | bytes accessed | tf_op | source)
XLA Modules:
  0.0 94.9 jit_solution(364573543193745845)
XLA Ops:
  0.6 0.0 copy-start.14
  0.6 0.0 copy-start.9
  0.7 0.0 copy-start.12
  0.7 0.0 copy-start.11
  0.7 0.0 copy-start.10
  0.7 0.0 copy-start.7
  0.7 0.0 copy-start.5
  0.7 0.0 copy-start.6
  0.7 0.0 copy-start.4
  0.7 0.0 copy-start.1
  0.7 1.9 %broadcast_in_dim.34 = bf16[64,512,16]{1,2,0:T(8,128)(2,1)} broadcast(bf16[512,16]{0,1:T(8,128)(2,1)} %param.29), dimensions={1,2} | broadcast | bytes 1064960 | tf_op jit(solution)/shard_map/broadcast_in_dim | solution.py:16
  2.6 18.8 %all-to-all-start = ((bf16[64,512,16]{1,2,0:T(8,128)(2,1)}), bf16[64,512,16]{1,2,0:T(8,128)(2,1)S(1)}, u32[]{:S(2)}, u32[]{:S(2)}) async-start(bf16[64,512,16]{1,2,0:T(8,128)(2,1)} %broadcast_in_dim.34), calls=%async_computation | async-start | bytes 2097152 | tf_op jit(solution)/shard_map/all_to_all | solution.py:15
  21.4 0.0 copy-done.12
  21.4 0.0 copy-done.11
  21.6 0.1 copy.77
  21.6 0.1 copy.81
  21.7 0.1 fusion.4
  21.8 0.1 copy.82
  21.9 0.0 copy-done.7
  21.9 0.1 copy.89
  22.1 0.0 copy-start.13
  22.1 0.2 fusion.26
  22.3 0.1 copy.93
  22.4 0.2 fusion.6
  22.7 0.1 copy.104
  22.8 0.1 copy.123
  22.9 0.1 copy.124
  23.0 0.0 copy-done.2
  23.0 0.3 fusion.10
  23.3 0.0 copy-done
  23.3 1.1 %fusion.8 = f32[8,2,8,256]{3,2,1,0:T(8,128)S(1)} fusion(f32[8,2,128,256]{3,2,1,0:T(8,128)S(1)} %copy-done, f32[8,2,8,128]{3,0,1,2:T(8,128)S(1)} %pad_bitcast_fusion), kind=kOutput, calls=%fused_computation.18 | convolution fusion | flops 50331648 | bytes 2293760 | tf_op jit(solution)/shard_map/vmap(hld,hde->hle)/dot_general | solution.py:55
  24.4 0.2 fusion.24
  24.6 0.2 multiply_reduce_fusion
  24.9 0.1 fusion.11
  25.0 0.1 copy.100
  25.1 0.1 copy.99
  25.2 0.1 copy.106
  25.3 0.2 fusion.13
  25.5 2.7 %multiply_add_fusion = f32[8,2,128,256]{3,2,1,0:T(8,128)} fusion(f32[8,2,128,256]{3,2,1,0:T(8,128)S(1)} %copy-done, f32[8,2]{1,0:T(8,128)S(1)} %copy.99, bf16[8,4,2,256]{3,1,2,0:T(4,128)(2,1)S(1)} %copy.91, bf16[8,4,2,256]{3,1,2,0:T(4,128)(2,1)S(1)} %copy.90, f32[8,2,8]{2,1,0:T(2,128)S(1)} %copy.100, bf16[8,4,2,128]{3,1,2,0:T(4,128)(2,1)S(1)} %copy.87, ...), kind=kOutput, calls=%fused_computation.2 | convolution fusion | flops 51609600 | bytes 4293184 | tf_op jit(solution)/shard_map/vmap(hld,hle->hde)/dot_general | solution.py:65
  28.2 48.4 %all-to-all-done = bf16[64,512,16]{1,2,0:T(8,128)(2,1)S(1)} async-done(((bf16[64,512,16]{1,2,0:T(8,128)(2,1)}), bf16[64,512,16]{1,2,0:T(8,128)(2,1)S(1)}, u32[]{:S(2)}, u32[]{:S(2)}) %all-to-all-start) | async-done | bytes 1048608 | tf_op jit(solution)/shard_map/all_to_all | solution.py:15
  76.6 0.3 broadcast_in_dim.35
  76.9 5.4 %all_to_all.15 = bf16[2,64,512,16]{2,3,1,0:T(8,128)(2,1)S(1)} all-to-all(bf16[2,64,512,16]{2,3,1,0:T(8,128)(2,1)S(1)} %broadcast_in_dim.35), channel_id=1, replica_groups=mesh['kv_0'=16,'kv_1'=4,'kv_2'=2,'tp'=4] {'kv_2'}, dimensions={0} | all-to-all | bytes 4194304 | tf_op jit(solution)/shard_map/all_to_all | solution.py:15
  82.3 0.2 copy.96
  82.5 1.4 %fusion = bf16[4,8,1,2048]{3,1,2,0:T(8,128)(2,1)} fusion(bf16[8,4,512]{2,0,1:T(8,128)(2,1)S(1)} %convert_element_type.22, bf16[512,2048,1]{0,1,2:T(8,128)(2,1)S(1)} %bitcast.62), kind=kOutput, calls=%fused_computation.1 | convolution fusion | flops 67174400 | bytes 2260992 | tf_op jit(solution)/shard_map/spr,rc->spc/dot_general | solution.py:156
  83.8 4.5 %all-to-all-start.2 = ((bf16[4,8,1,2048]{3,1,2,0:T(8,128)(2,1)}), bf16[4,8,1,2048]{3,1,2,0:T(8,128)(2,1)S(1)}, u32[]{:S(2)}, u32[]{:S(2)}) async-start(bf16[4,8,1,2048]{3,1,2,0:T(8,128)(2,1)} %fusion), calls=%async_computation.2 | async-start | bytes 262144 | tf_op jit(solution)/shard_map/all_to_all | solution.py:40
  88.3 0.7 multiply_add_fusion.1
  89.0 5.3 %all-to-all-done.2 = bf16[4,8,1,2048]{3,1,2,0:T(8,128)(2,1)S(1)} async-done(((bf16[4,8,1,2048]{3,1,2,0:T(8,128)(2,1)}), bf16[4,8,1,2048]{3,1,2,0:T(8,128)(2,1)S(1)}, u32[]{:S(2)}, u32[]{:S(2)}) %all-to-all-start.2) | async-done | bytes 131104 | tf_op jit(solution)/shard_map/all_to_all | solution.py:40
  94.3 0.6 reduce_sum.44
  (38 shorter events, 0.3 us)
Async XLA Ops:
  0.6 20.8 %copy-start.14 = (s32[8]{0:T(128)S(1)}, s32[8]{0:T(128)}, u32[]{:S(2)}) copy-start(s32[8]{0:T(128)} %param.24) | copy-start | bytes 100
  0.6 20.8 %copy-start.9 = (f32[8,4,2]{0,2,1:T(2,128)S(1)}, f32[8,4,2]{0,2,1:T(2,128)}, u32[]{:S(2)}) copy-start(f32[8,4,2]{0,2,1:T(2,128)} %param.18) | copy-start | bytes 772
  0.7 20.8 %copy-start.12 = (f32[8,4,2]{0,2,1:T(2,128)S(1)}, f32[8,4,2]{0,2,1:T(2,128)}, u32[]{:S(2)}) copy-start(f32[8,4,2]{0,2,1:T(2,128)} %param.22) | copy-start | bytes 772
  0.7 20.8 %copy-start.11 = (f32[8,4,2]{0,2,1:T(2,128)S(1)}, f32[8,4,2]{0,2,1:T(2,128)}, u32[]{:S(2)}) copy-start(f32[8,4,2]{0,2,1:T(2,128)} %param.23) | copy-start | bytes 772
  0.7 20.8 %copy-start.10 = (f32[8,4,2]{0,2,1:T(2,128)S(1)}, f32[8,4,2]{0,2,1:T(2,128)}, u32[]{:S(2)}) copy-start(f32[8,4,2]{0,2,1:T(2,128)} %param.19) | copy-start | bytes 772
  0.7 21.2 %copy-start.7 = (f32[8,2]{0,1:T(2,128)S(1)}, f32[8,2]{0,1:T(2,128)}, u32[]{:S(2)}) copy-start(f32[8,2]{0,1:T(2,128)} %param.27) | copy-start | bytes 196
  0.7 21.3 %copy-start.5 = (bf16[8,4,2,128]{3,2,1,0:T(2,128)(2,1)S(1)}, bf16[8,4,2,128]{3,2,1,0:T(2,128)(2,1)}, u32[]{:S(2)}) copy-start(bf16[8,4,2,128]{3,2,1,0:T(2,128)(2,1)} %param.20) | copy-start | bytes 49156
  0.7 21.4 %copy-start.6 = (bf16[8,4,2,128]{3,2,1,0:T(2,128)(2,1)S(1)}, bf16[8,4,2,128]{3,2,1,0:T(2,128)(2,1)}, u32[]{:S(2)}) copy-start(bf16[8,4,2,128]{3,2,1,0:T(2,128)(2,1)} %param.16) | copy-start | bytes 49156
  0.7 21.4 %copy-start.4 = (bf16[8,4,2,128]{3,2,1,0:T(2,128)(2,1)S(1)}, bf16[8,4,2,128]{3,2,1,0:T(2,128)(2,1)}, u32[]{:S(2)}) copy-start(bf16[8,4,2,128]{3,2,1,0:T(2,128)(2,1)} %param.15) | copy-start | bytes 49156
  0.7 21.7 %copy-start.1 = (f32[8,2,128]{2,1,0:T(2,128)S(1)}, f32[8,2,128]{2,1,0:T(2,128)}, u32[]{:S(2)}) copy-start(f32[8,2,128]{2,1,0:T(2,128)} %param.26) | copy-start | bytes 24580
  2.6 20.4 %copy-start.2 = (bf16[8,4,2,256]{3,2,1,0:T(2,128)(2,1)S(1)}, bf16[8,4,2,256]{3,2,1,0:T(2,128)(2,1)}, u32[]{:S(2)}) copy-start(bf16[8,4,2,256]{3,2,1,0:T(2,128)(2,1)} %param.21) | copy-start | bytes 98308
  2.6 20.4 %copy-start.3 = (bf16[8,4,2,256]{3,2,1,0:T(2,128)(2,1)S(1)}, bf16[8,4,2,256]{3,2,1,0:T(2,128)(2,1)}, u32[]{:S(2)}) copy-start(bf16[8,4,2,256]{3,2,1,0:T(2,128)(2,1)} %param.17) | copy-start | bytes 98308
  2.6 20.7 %copy-start = (f32[8,2,128,256]{3,2,1,0:T(8,128)S(1)}, f32[8,2,128,256]{3,2,1,0:T(8,128)}, u32[]{:S(2)}) copy-start(f32[8,2,128,256]{3,2,1,0:T(8,128)} %param.25) | copy-start | bytes 6291460
  2.6 74.0 %all-to-all-start = ((bf16[64,512,16]{1,2,0:T(8,128)(2,1)}), bf16[64,512,16]{1,2,0:T(8,128)(2,1)S(1)}, u32[]{:S(2)}, u32[]{:S(2)}) async-start(bf16[64,512,16]{1,2,0:T(8,128)(2,1)} %broadcast_in_dim.34), calls=%async_computation | async-start | bytes 2097152 | tf_op jit(solution)/shard_map/all_to_all | solution.py:15
  22.0 3.1 %copy-start.8 = (f32[8,2,1]{0,2,1:T(1,128)}, f32[8,2,1]{0,2,1:T(1,128)S(1)}, u32[]{:S(2)}) copy-start(f32[8,2,1]{0,2,1:T(1,128)S(1)} %slice.18) | copy-start | bytes 196
  22.1 2.7 %copy-start.13 = (f32[2,256]{1,0:T(2,128)S(1)}, f32[2,256]{1,0:T(2,128)}, u32[]{:S(2)}) copy-start(f32[2,256]{1,0:T(2,128)} %param.28) | copy-start | bytes 6148
  83.8 10.4 %all-to-all-start.2 = ((bf16[4,8,1,2048]{3,1,2,0:T(8,128)(2,1)}), bf16[4,8,1,2048]{3,1,2,0:T(8,128)(2,1)S(1)}, u32[]{:S(2)}, u32[]{:S(2)}) async-start(bf16[4,8,1,2048]{3,1,2,0:T(8,128)(2,1)} %fusion), calls=%async_computation.2 | async-start | bytes 262144 | tf_op jit(solution)/shard_map/all_to_all | solution.py:40
where the time goes:
time: 95.3 us; the launch traced here: 94.9 us
  waiting for transfers between devices  53.7 us (56%)
  starting transfers between devices  23.2 us (24%)
  matrix products  6.09 us (6%)
  blocking collectives  5.42 us (6%)
  local copies, waits for them, and re-layouts  3.42 us (4%)
  other arithmetic  2.04 us (2%)
  between operations  1.03 us (1%)
    all_to_all x1, waiting for transfers between devices, sent_to_all(): lax.all_to_all(jnp.broadcast_to(shard[None], (size, *shard.shape)), axis,...  48.4 us
    all_to_all x1, starting transfers between devices, sent_to_all(): lax.all_to_all(jnp.broadcast_to(shard[None], (size, *shard.shape)), axis,...  18.8 us
    all_to_all x1, blocking collectives, sent_to_all(): lax.all_to_all(jnp.broadcast_to(shard[None], (size, *shard.shape)), axis,...  5.42 us
    all_to_all x1, waiting for transfers between devices, summed_on_arrival(): lax.all_to_all(pieces, axis, split_axis=0, concat_axis=0, tiled=True)  5.3 us
    all_to_all x1, starting transfers between devices, summed_on_arrival(): lax.all_to_all(pieces, axis, split_axis=0, concat_axis=0, tiled=True)  4.46 us
    dot_general x1, matrix products, cell(): jnp.einsum('hld,hle->hde', g_tok[..., None] * keys, values, precision=HIGH)  2.7 us
    broadcast_in_dim x2, local copies, waits for them, and re-layouts, sent_to_all(): jnp.broadcast_to(shard[None], (size, *shard.shape))  2.15 us
  transfers between devices with their start and end apart: 2, of which 2 were waited for; matrix products, arithmetic and copies ran while one was open for 8% of the time, Pallas kernels for 0%

commit v1 on v0

v1 whole, which is shorter than its diff:
```python
import jax
import jax.numpy as jnp
from jax import lax
from jax.experimental import pallas as pl
from jax.experimental.pallas import tpu as pltpu
from jax.sharding import Mesh
from jax.sharding import PartitionSpec as P

KV = ("kv_0", "kv_1", "kv_2")
PLANE = ("kv_1", "kv_2")

SEQS = 8
PROPS = 4
HEADS = 2
DK = 128
DV = 256
ROWS = SEQS * PROPS * HEADS
RUN = 2 * ROWS
ITEMS = SEQS * HEADS
CHUNK = 4
CHUNKS = ITEMS // CHUNK
EPS = 1e-5


def iota(shape, dim):
    return lax.broadcasted_iota(jnp.int32, shape, dim)


def item_of(row):
    return (row // 8) % 8 * 2 + row % 2


def place_of(row):
    return row // 64 * 4 + row // 2 % 4


def exact_dot(a, b):
    return jnp.dot(a, b, precision=lax.Precision.HIGHEST, preferred_element_type=jnp.float32)


def halves(x):
    high = x.astype(jnp.bfloat16)
    return high, (x - high.astype(jnp.float32)).astype(jnp.bfloat16)


def dot_bt(a, b):
    return lax.dot_general(a, b, (((1,), (1,)), ((), ())), preferred_element_type=jnp.float32)


def log_sigmoid(x):
    return jnp.minimum(x, 0.0) - jnp.log1p(jnp.exp(-jnp.abs(x)))


def state_copies(state_hbm, state, sems):
    return [
        pltpu.make_async_copy(
            state_hbm.at[pl.ds(c * CHUNK, CHUNK)], state.at[pl.ds(c * CHUNK, CHUNK)], sems.at[c]
        )
        for c in range(CHUNKS)
    ]


def hidden_kernel(
    q_ref, k_ref, ko_ref, v_ref, vo_ref, ig_ref, fg_ref, igo_ref, fgo_ref, acc_ref, smax_ref,
    norm_ref, gain_ref, state_hbm, hidden_ref, coef_ref, state, flat, sems,
):
    copies = state_copies(state_hbm, state, sems)
    for copy in copies:
        copy.start()

    lane1 = iota((1, RUN), 1)
    parts = []
    for ref in (igo_ref, ig_ref, fgo_ref, fg_ref):
        parts.append(jnp.concatenate([ref[p] for p in range(PROPS)], axis=0))
    parts.append(
        jnp.concatenate(
            [smax_ref[...], acc_ref[...].astype(jnp.float32), jnp.zeros((5, SEQS), jnp.float32)],
            axis=0,
        )
    )
    spread = (iota((SEQS, RUN), 1) % 64 // 8 == iota((SEQS, RUN), 0)).astype(jnp.float32)
    wide = exact_dot(jnp.concatenate(parts, axis=0), spread)
    own = iota((8, RUN), 0) == iota((8, RUN), 1) % 8
    rows = [
        jnp.sum(jnp.where(own, wide[8 * a : 8 * a + 8], 0.0), axis=0, keepdims=True)
        for a in range(4)
    ]
    smax = jnp.where(lane1 % 2 == 0, wide[32:33], wide[33:34])
    old = lane1 < ROWS
    live = (lane1 // 2 % 4).astype(jnp.float32) < wide[34:35]
    ig = jnp.where(old, jnp.where(live, rows[0], -jnp.inf), rows[1])
    forget = log_sigmoid(jnp.where(old, rows[2], rows[3]))
    forget = jnp.where(old & ~live, 0.0, forget)

    src, dst = iota((RUN, RUN), 0), iota((RUN, RUN), 1)
    together = item_of(src) == item_of(dst)
    upto = (together & (place_of(src) <= place_of(dst))).astype(jnp.float32)
    sums = exact_dot(
        jnp.broadcast_to(forget, (8, RUN)),
        jnp.concatenate([upto, together.astype(jnp.float32)], axis=1),
    )
    b = sums[0:1, :RUN]
    b_last = sums[0:1, RUN:]

    qrow, lane = iota((ROWS, RUN), 0), iota((ROWS, RUN), 1)
    same = item_of(qrow) == item_of(lane)
    valid = same & (place_of(lane) <= PROPS + qrow // 2 % 4)
    at = lane == ROWS + qrow
    b_col = jnp.sum(jnp.where(at, b, 0.0), axis=1, keepdims=True)
    inter = jnp.sum(jnp.where(at, b + smax, 0.0), axis=1, keepdims=True)
    logd = jnp.where(valid, b_col + (ig - b), -jnp.inf)
    m_row = jnp.maximum(inter, jnp.max(logd, axis=1, keepdims=True))
    decay = jnp.exp(logd - m_row)
    w_inter = jnp.exp(inter - m_row)

    last = same & (qrow // 2 % 4 == PROPS - 1)
    new_max = jnp.sum(jnp.where(last, m_row, 0.0), axis=0, keepdims=True)
    coef_ref[0:1, :] = jnp.exp(b_last - b + ig - new_max)
    coef_ref[1:2, :] = jnp.exp(b_last + smax - new_max)
    coef_ref[2:3, :] = new_max
    coef_ref[3:8, :] = jnp.zeros((5, RUN), jnp.float32)

    scale = DK**-0.5
    q = q_ref[...]
    k = jnp.concatenate([ko_ref[...], k_ref[...]], axis=0)
    v = jnp.concatenate([vo_ref[...], v_ref[...]], axis=0)
    probs = dot_bt(q, k) * scale * decay
    p_high, p_low = halves(probs)
    intra = jnp.dot(p_high, v, preferred_element_type=jnp.float32) + jnp.dot(
        p_low, v, preferred_element_type=jnp.float32
    )
    qn = lax.dot_general(
        q.astype(jnp.float32), norm_ref[...], (((1,), (1,)), ((), ())),
        precision=lax.Precision.HIGHEST, preferred_element_type=jnp.float32,
    )
    mine = item_of(iota((ROWS, ITEMS), 0)) == iota((ROWS, ITEMS), 1)
    qn = jnp.sum(jnp.where(mine, qn, 0.0), axis=1, keepdims=True)
    w_scaled = w_inter * scale
    den = w_scaled * qn + jnp.sum(probs, axis=1, keepdims=True)
    inv = 1.0 / jnp.maximum(jnp.abs(den), 1.0)
    gain = jnp.where(iota((ROWS // CHUNKS, DV), 0) % 2 == 0, gain_ref[0:1, :], gain_ref[1:2, :])

    size = ROWS // CHUNKS
    for c in range(CHUNKS):
        lo, hi = c * size, (c + 1) * size
        qc = q[lo:hi].astype(jnp.float32)
        item = item_of(iota((size, DK), 0) + lo)
        lhs = jnp.concatenate(
            [jnp.where(item == c * CHUNK + i, qc, 0.0) for i in range(CHUNK)], axis=1
        ).astype(jnp.bfloat16)
        copies[c].wait()
        s_high, s_low = halves(state[pl.ds(c * CHUNK, CHUNK)].reshape(CHUNK * DK, DV))
        num = jnp.dot(lhs, s_high, preferred_element_type=jnp.float32) + jnp.dot(
            lhs, s_low, preferred_element_type=jnp.float32
        )
        h = (w_scaled[lo:hi] * num + intra[lo:hi]) * inv[lo:hi]
        h = h - jnp.mean(h, axis=1, keepdims=True)
        var = jnp.mean(h * h, axis=1, keepdims=True)
        h = h * lax.rsqrt(var + EPS) * gain
        for half in range(2):
            flat[half, lo:hi, :] = h[:, half * DK : (half + 1) * DK]
    for p in range(PROPS):
        for head in range(HEADS):
            for half in range(2):
                piece = flat[half, pl.ds(p * HEADS + head, SEQS, stride=8), :]
                at = head * DV + half * DK
                hidden_ref[p, :, at : at + DK] = piece.astype(jnp.bfloat16)


def memory_kernel(
    coef_ref, k_ref, ko_ref, v_ref, vo_ref, norm_ref, state_hbm,
    new_hbm, new_norm_ref, state, new, sems, out_sems,
):
    copies = state_copies(state_hbm, state, sems)
    for copy in copies:
        copy.start()
    tok, keep = coef_ref[0:1, :], coef_ref[1:2, :]
    k = jnp.concatenate([ko_ref[...], k_ref[...]], axis=0).astype(jnp.float32)
    v = jnp.concatenate([vo_ref[...], v_ref[...]], axis=0)
    lane = iota((ITEMS, RUN), 1)
    mine = item_of(lane) == iota((ITEMS, RUN), 0)
    t_high, t_low = halves(jnp.where(mine, tok, 0.0))
    kb = k.astype(jnp.bfloat16)
    kept = jnp.sum(jnp.where(mine & (place_of(lane) == 0), keep, 0.0), axis=1, keepdims=True)
    new_norm_ref[...] = (
        kept * norm_ref[...]
        + jnp.dot(t_high, kb, preferred_element_type=jnp.float32)
        + jnp.dot(t_low, kb, preferred_element_type=jnp.float32)
    )
    weighted = k.T * tok
    twice = jnp.concatenate([v, v], axis=0)
    lane = item_of(iota((DK, RUN), 1))
    stores = []
    for c in range(CHUNKS):
        copies[c].wait()
        for i in range(c * CHUNK, (c + 1) * CHUNK):
            high, low = halves(jnp.where(lane == i, weighted, 0.0))
            update = jnp.dot(
                jnp.concatenate([high, low], axis=1), twice, preferred_element_type=jnp.float32
            )
            at = i // 2 * 8 + i % 2
            new[i] = keep[:, at : at + 1] * state[i] + update
        stores.append(
            pltpu.make_async_copy(
                new.at[pl.ds(c * CHUNK, CHUNK)], new_hbm.at[pl.ds(c * CHUNK, CHUNK)], out_sems.at[c]
            )
        )
        stores[-1].start()
    for store in stores:
        store.wait()


VMEM = pl.BlockSpec(memory_space=pltpu.VMEM)
ANY = pl.BlockSpec(memory_space=pl.ANY)


def hidden_of(q, k, ko, v, vo, ig, fg, igo, fgo, accepted, smax, norm, gain, state):
    return pl.pallas_call(
        hidden_kernel,
        in_specs=[VMEM] * 13 + [ANY],
        out_specs=(VMEM, VMEM),
        out_shape=(
            jax.ShapeDtypeStruct((PROPS, SEQS, HEADS * DV), jnp.bfloat16),
            jax.ShapeDtypeStruct((8, RUN), jnp.float32),
        ),
        scratch_shapes=[
            pltpu.VMEM((ITEMS, DK, DV), jnp.float32),
            pltpu.VMEM((2, ROWS, DK), jnp.float32),
            pltpu.SemaphoreType.DMA((CHUNKS,)),
        ],
        name="hidden",
    )(q, k, ko, v, vo, ig, fg, igo, fgo, accepted, smax, norm, gain, state)


def memory_of(coef, k, ko, v, vo, norm, state):
    return pl.pallas_call(
        memory_kernel,
        in_specs=[VMEM] * 6 + [ANY],
        out_specs=(ANY, VMEM),
        out_shape=(
            jax.ShapeDtypeStruct((ITEMS, DK, DV), jnp.float32),
            jax.ShapeDtypeStruct((ITEMS, DK), jnp.float32),
        ),
        scratch_shapes=[
            pltpu.VMEM((ITEMS, DK, DV), jnp.float32),
            pltpu.VMEM((ITEMS, DK, DV), jnp.float32),
            pltpu.SemaphoreType.DMA((CHUNKS,)),
            pltpu.SemaphoreType.DMA((CHUNKS,)),
        ],
        name="memory",
    )(coef, k, ko, v, vo, norm, state)


def to_each(block, count):
    return jnp.broadcast_to(block[None], (count, *block.shape))


def exchanged(pieces, axes):
    return lax.all_to_all(pieces, axes, split_axis=0, concat_axis=0, tiled=True)


def on_device(
    queries,
    keys,
    values,
    in_gate,
    forget_pre,
    old_keys,
    old_values,
    old_in_gate,
    old_forget,
    accepted,
    state_mem,
    state_norm,
    state_max,
    norm_gain,
    out_weight,
):
    zs, cross, tps = lax.axis_size("kv_0"), lax.axis_size(PLANE), lax.axis_size("tp")
    weight = exchanged(to_each(out_weight.T, zs), "kv_0")
    weight = weight.reshape(-1, out_weight.shape[0])
    q, k, ko, v, vo = (
        a.reshape(ROWS, -1) for a in (queries, keys, old_keys, values, old_values)
    )
    gates = (
        a.transpose(1, 2, 0) for a in (in_gate, forget_pre, old_in_gate, old_forget)
    )
    norm = state_norm.reshape(ITEMS, DK)
    state = state_mem.reshape(ITEMS, DK, DV)
    hidden, coef = hidden_of(
        q, k, ko, v, vo, *gates, accepted[None], state_max.T, norm, norm_gain, state
    )
    rows = lax.all_gather(hidden.reshape(PROPS * SEQS, -1), PLANE, tiled=True)
    new_mem, new_norm = memory_of(coef, k, ko, v, vo, norm, state)
    terms = lax.dot_general(
        rows, weight, (((1,), (1,)), ((), ())), preferred_element_type=jnp.float32
    ).astype(jnp.bfloat16)
    terms = exchanged(terms.reshape(cross * tps, SEQS, -1), (*PLANE, "tp"))
    total = terms.astype(jnp.float32).reshape(cross, tps, SEQS, zs, -1).sum(axis=1)
    mixed = total.astype(jnp.bfloat16).transpose(1, 2, 0, 3).reshape(SEQS, 1, -1)
    new_max = coef[2, :ROWS].reshape(SEQS, PROPS, HEADS)[:, 0]
    return (
        mixed,
        new_mem.reshape(state_mem.shape),
        new_norm.reshape(state_norm.shape),
        new_max,
    )


def solution(mesh):
    finer = Mesh(mesh.devices.reshape(16, 4, 2, mesh.shape["tp"]), (*KV, "tp"))
    in_specs = (
        P(KV, None, "tp", None),
        P(KV, None, "tp", None),
        P(KV, None, "tp", None),
        P(KV, None, "tp"),
        P(KV, None, "tp"),
        P(KV, None, "tp", None),
        P(KV, None, "tp", None),
        P(KV, None, "tp"),
        P(KV, None, "tp"),
        P(KV),
        P(KV, "tp", None, None),
        P(KV, "tp", None),
        P(KV, "tp"),
        P("tp", None),
        P("tp", KV),
    )
    out_specs = (P(KV, "tp", None), P(KV, "tp", None, None), P(KV, "tp", None), P(KV, "tp"))
    return jax.shard_map(
        on_device, mesh=finer, in_specs=in_specs, out_specs=out_specs, check_vma=False
    )
```

time: 95.3 us -> 57 us (0.60)
  the two profiles are of different devices: /device:TPU:2 before, /device:TPU:1 now
where the time goes in v1:
time: 57 us; the launch traced here: 56.3 us
  starting transfers between devices  22.4 us (39%)
  blocking collectives  14.2 us (25%)
  Pallas kernels  8.59 us (15%)
  local copies, waits for them, and re-layouts  7.48 us (13%)
  waiting for transfers between devices  1.82 us (3%)
  matrix products  0.92 us (2%)
  between operations  0.7 us (1%)
    all_to_all x2, starting transfers between devices, exchanged(): return lax.all_to_all(pieces, axes, split_axis=0, concat_axis=0, tiled=True)  22.4 us
    all_gather x1, blocking collectives, on_device(): rows = lax.all_gather(hidden.reshape(PROPS * SEQS, -1), PLANE, tiled=True)  14.2 us
    pallas_call x1, Pallas kernels, hidden_of(): pl.pallas_call(hidden_kernel, in_specs=[VMEM] * 13 + [ANY], out_specs=(VM...  4.32 us
    pallas_call x1, Pallas kernels, memory_of(): pl.pallas_call(memory_kernel, in_specs=[VMEM] * 6 + [ANY], out_specs=(ANY...  4.27 us
    reshape x2, local copies, waits for them, and re-layouts, on_device(): a.reshape(ROWS, -1)  2.77 us
    all_to_all x2, waiting for transfers between devices, exchanged(): return lax.all_to_all(pieces, axes, split_axis=0, concat_axis=0, tiled=True)  1.82 us
    broadcast_in_dim x1, local copies, waits for them, and re-layouts, to_each(): return jnp.broadcast_to(block[None], (count, *block.shape))  1.45 us
    slice x3, local copies, waits for them, and re-layouts, on_device(): new_max = coef[2, :ROWS].reshape(SEQS, PROPS, HEADS)[:, 0]  1.35 us
  transfers between devices with their start and end apart: 2, of which 1 were waited for; matrix products, arithmetic and copies ran while one was open for 8% of the time, Pallas kernels for 15%

profile of v1, /device:TPU:1, one launch (start us, length us, event | category | flops | bytes accessed | tf_op | source)
XLA Modules:
  0.0 56.3 jit_solution(14732125669442249708)
XLA Ops:
  0.6 1.4 %broadcast_in_dim.10 = bf16[16,16,512]{2,1,0:T(8,128)(2,1)} broadcast(bf16[16,512]{1,0:T(8,128)(2,1)} %bitcast.36), dimensions={1,2} | broadcast | bytes 278528 | tf_op jit(solution)/shard_map/broadcast_in_dim | solution.py:255
  2.1 15.7 %all-to-all-start = ((bf16[16,16,512]{2,1,0:T(8,128)(2,1)}), bf16[16,16,512]{2,1,0:T(8,128)(2,1)S(1)}, u32[]{:S(2)}, u32[]{:S(2)}) async-start(bf16[16,16,512]{2,1,0:T(8,128)(2,1)} %broadcast_in_dim.10), calls=%async_computation | async-start | bytes 524288 | tf_op jit(solution)/shard_map/all_to_all | solution.py:259
  17.8 1.4 %reshape.57.v_ref = bf16[64,256]{1,0:T(8,128)(2,1)} reshape(bf16[8,4,2,256]{3,2,1,0:T(2,128)(2,1)} %param.17) | data formatting | bytes 65536 | tf_op jit(solution)/shard_map/reshape | solution.py:283
  19.2 1.4 %reshape.58.vo_ref = bf16[64,256]{1,0:T(8,128)(2,1)} reshape(bf16[8,4,2,256]{3,2,1,0:T(2,128)(2,1)} %param.21) | data formatting | bytes 65536 | tf_op jit(solution)/shard_map/reshape | solution.py:283
  20.6 4.3 %hidden.1 = (bf16[4,8,512]{2,1,0:T(8,128)(2,1)}, f32[8,128]{1,0:T(8,128)}) custom-call(bf16[64,128]{1,0:T(8,128)(2,1)} %bitcast.35, bf16[64,128]{1,0:T(8,128)(2,1)} %bitcast.28, bf16[64,128]{1,0:T(8,128)(2,1)} %bitcast.30, bf16[64,256]{1,0:T(8,128)(2,1)} %reshape.57.v_ref, bf16[64,256]{1,0:T(8,128)(2,1)} %reshape.58.vo_ref, f32[4,2,8]{2,1,0:T(2,128)} %bitcast.37, ...), custom_call_target="tpu_custom_call" | custom-call | tf_op jit(solution)/shard_map/hidden/pallas_call | solution.py:218
  24.9 14.2 %all_gather.3 = bf16[256,512]{1,0:T(8,128)(2,1)S(1)} all-gather(bf16[32,512]{1,0:T(8,128)(2,1)} %bitcast.34), channel_id=1, replica_groups=mesh['kv_0'=16,'kv_1'=4,'kv_2'=2,'tp'=4] {'kv_1','kv_2'}, dimensions={0}, use_global_device_ids=true | all-gather | bytes 294912 | tf_op jit(solution)/shard_map/all_gather | solution.py:293
  39.1 0.0 all-to-all-done
  39.1 0.9 %fusion = bf16[32,8,256]{2,1,0:T(8,128)(2,1)} fusion(bf16[256,512]{1,0:T(8,128)(2,1)S(1)} %all_gather.3, bf16[256,512]{1,0:T(8,128)(2,1)S(1)} %bitcast.27), kind=kOutput, calls=%fused_computation.1 | convolution fusion | flops 67174400 | bytes 655360 | tf_op jit(solution)/shard_map/dot_general | solution.py:295
  40.0 6.6 %all-to-all-start.1 = ((bf16[32,8,256]{2,1,0:T(8,128)(2,1)}), bf16[32,8,256]{2,1,0:T(8,128)(2,1)S(1)}, u32[]{:S(2)}, u32[]{:S(2)}) async-start(bf16[32,8,256]{2,1,0:T(8,128)(2,1)} %fusion), calls=%async_computation.1 | async-start | bytes 262144 | tf_op jit(solution)/shard_map/all_to_all | solution.py:259
  46.7 4.3 %memory.1 = (f32[16,128,256]{2,1,0:T(8,128)}, f32[16,128]{1,0:T(8,128)}) custom-call(f32[8,128]{1,0:T(8,128)} %get-tuple-element.9.coef_ref, bf16[64,128]{1,0:T(8,128)(2,1)} %bitcast.29, bf16[64,128]{1,0:T(8,128)(2,1)} %bitcast.31, bf16[64,256]{1,0:T(8,128)(2,1)} %reshape.57.v_ref, bf16[64,256]{1,0:T(8,128)(2,1)} %reshape.58.vo_ref, f32[16,128]{1,0:T(8,128)} %bitcast.33, ...), custom_call_target="tpu_custom_call" | custom-call | tf_op jit(solution)/shard_map/memory/pallas_call | solution.py:236
  50.9 0.7 %slice_reduce_fusion = f32[64]{0:T(128)S(1)} fusion(f32[8,128]{1,0:T(8,128)} %get-tuple-element.9.coef_ref), kind=kLoop, calls=%fused_computation.2 | loop fusion | bytes 512 | tf_op jit(solution)/shard_map/slice | solution.py:301
  51.6 0.1 reshape_squeeze.3
  51.8 0.6 %copy.23 = f32[8,1,2]{0,2,1:T(2,128)} copy(f32[8,1,2]{2,1,0:T(1,128)S(1)} %slice.8) | data formatting | bytes 128 | tf_op jit(solution)/shard_map/slice | solution.py:301
  52.4 1.8 %all-to-all-done.1 = bf16[32,8,256]{2,1,0:T(8,128)(2,1)S(1)} async-done(((bf16[32,8,256]{2,1,0:T(8,128)(2,1)}), bf16[32,8,256]{2,1,0:T(8,128)(2,1)S(1)}, u32[]{:S(2)}, u32[]{:S(2)}) %all-to-all-start.1) | async-done | bytes 131104 | tf_op jit(solution)/shard_map/all_to_all | solution.py:259
  54.2 0.7 %reshape.64 = bf16[8,4,8,16,16]{4,3,2,1,0:T(8,128)(2,1)S(1)} reshape(bf16[32,8,256]{2,1,0:T(8,128)(2,1)S(1)} %all-to-all-done.1) | data formatting | bytes 262144 | tf_op jit(solution)/shard_map/reshape | solution.py:299
  54.9 0.3 reduce
  55.2 0.2 copy.22
  55.4 0.9 %reshape.66 = bf16[8,1,2048]{2,0,1:T(8,128)(2,1)} reshape(bf16[8,16,8,16]{3,2,1,0:T(8,128)(2,1)S(1)} %copy.22) | data formatting | bytes 65536 | tf_op jit(solution)/shard_map/reshape | solution.py:300
  (1 shorter events, 0.0 us)
Async XLA Ops:
  2.1 37.0 %all-to-all-start = ((bf16[16,16,512]{2,1,0:T(8,128)(2,1)}), bf16[16,16,512]{2,1,0:T(8,128)(2,1)S(1)}, u32[]{:S(2)}, u32[]{:S(2)}) async-start(bf16[16,16,512]{2,1,0:T(8,128)(2,1)} %broadcast_in_dim.10), calls=%async_computation | async-start | bytes 524288 | tf_op jit(solution)/shard_map/all_to_all | solution.py:259
  40.0 14.2 %all-to-all-start.1 = ((bf16[32,8,256]{2,1,0:T(8,128)(2,1)}), bf16[32,8,256]{2,1,0:T(8,128)(2,1)S(1)}, u32[]{:S(2)}, u32[]{:S(2)}) async-start(bf16[32,8,256]{2,1,0:T(8,128)(2,1)} %fusion), calls=%async_computation.1 | async-start | bytes 262144 | tf_op jit(solution)/shard_map/all_to_all | solution.py:259

commit v2 on v1

--- a/solution.py
+++ b/solution.py
@@ -1,3 +1,5 @@
+import functools
+
 import jax
 import jax.numpy as jnp
 from jax import lax
@@ -51,6 +53,14 @@
     return jnp.minimum(x, 0.0) - jnp.log1p(jnp.exp(-jnp.abs(x)))
 
 
+def in_row_order(view):
+    dst, src = iota((RUN, RUN), 0), iota((RUN, RUN), 1)
+    row = dst % ROWS
+    pick = src == row // 2 * 4 + dst // ROWS * 2 + row % 2
+    rows = jnp.dot(pick.astype(jnp.bfloat16), view, preferred_element_type=jnp.float32)
+    return jnp.concatenate([rows[:ROWS], rows[ROWS:]], axis=1).astype(jnp.bfloat16)
+
+
 def state_copies(state_hbm, state, sems):
     return [
         pltpu.make_async_copy(
@@ -62,7 +72,7 @@
 
 def hidden_kernel(
     q_ref, k_ref, ko_ref, v_ref, vo_ref, ig_ref, fg_ref, igo_ref, fgo_ref, acc_ref, smax_ref,
-    norm_ref, gain_ref, state_hbm, hidden_ref, coef_ref, state, flat, sems,
+    norm_ref, gain_ref, state_hbm, hidden_ref, coef_ref, values_ref, state, flat, sems,
 ):
     copies = state_copies(state_hbm, state, sems)
     for copy in copies:
@@ -123,7 +133,8 @@
     scale = DK**-0.5
     q = q_ref[...]
     k = jnp.concatenate([ko_ref[...], k_ref[...]], axis=0)
-    v = jnp.concatenate([vo_ref[...], v_ref[...]], axis=0)
+    v = jnp.concatenate([in_row_order(vo_ref[...]), in_row_order(v_ref[...])], axis=0)
+    values_ref[...] = v
     probs = dot_bt(q, k) * scale * decay
     p_high, p_low = halves(probs)
     intra = jnp.dot(p_high, v, preferred_element_type=jnp.float32) + jnp.dot(
@@ -168,15 +179,19 @@
 
 
 def memory_kernel(
-    coef_ref, k_ref, ko_ref, v_ref, vo_ref, norm_ref, state_hbm,
-    new_hbm, new_norm_ref, state, new, sems, out_sems,
+    coef_ref, k_ref, ko_ref, values_ref, norm_ref, state_hbm,
+    new_hbm, new_norm_ref, new_max_ref, state, new, sems, out_sems,
 ):
     copies = state_copies(state_hbm, state, sems)
     for copy in copies:
         copy.start()
     tok, keep = coef_ref[0:1, :], coef_ref[1:2, :]
     k = jnp.concatenate([ko_ref[...], k_ref[...]], axis=0).astype(jnp.float32)
-    v = jnp.concatenate([vo_ref[...], v_ref[...]], axis=0)
+    v = values_ref[...]
+    lane = iota((8, RUN), 1)
+    first = (place_of(lane) == 0) & (lane % 2 == iota((8, RUN), 0))
+    seq = (iota((RUN, SEQS), 0) // 8 % 8 == iota((RUN, SEQS), 1)).astype(jnp.float32)
+    new_max_ref[...] = exact_dot(jnp.where(first, coef_ref[2:3, :], 0.0), seq)[:HEADS]
     lane = iota((ITEMS, RUN), 1)
     mine = item_of(lane) == iota((ITEMS, RUN), 0)
     t_high, t_low = halves(jnp.where(mine, tok, 0.0))
@@ -218,10 +233,11 @@
     return pl.pallas_call(
         hidden_kernel,
         in_specs=[VMEM] * 13 + [ANY],
-        out_specs=(VMEM, VMEM),
+        out_specs=(VMEM, VMEM, VMEM),
         out_shape=(
-            jax.ShapeDtypeStruct((PROPS, SEQS, HEADS * DV), jnp.bfloat16),
-            jax.ShapeDtypeStruct((8, RUN), jnp.float32),
+            pltpu.VMEM((PROPS, SEQS, HEADS * DV), jnp.bfloat16),
+            pltpu.VMEM((8, RUN), jnp.float32),
+            pltpu.VMEM((RUN, DV), jnp.bfloat16),
         ),
         scratch_shapes=[
             pltpu.VMEM((ITEMS, DK, DV), jnp.float32),
@@ -232,14 +248,15 @@
     )(q, k, ko, v, vo, ig, fg, igo, fgo, accepted, smax, norm, gain, state)
 
 
-def memory_of(coef, k, ko, v, vo, norm, state):
+def memory_of(coef, k, ko, v, norm, state):
     return pl.pallas_call(
         memory_kernel,
-        in_specs=[VMEM] * 6 + [ANY],
-        out_specs=(ANY, VMEM),
+        in_specs=[VMEM] * 5 + [ANY],
+        out_specs=(ANY, VMEM, VMEM),
         out_shape=(
             jax.ShapeDtypeStruct((ITEMS, DK, DV), jnp.float32),
             jax.ShapeDtypeStruct((ITEMS, DK), jnp.float32),
+            jax.ShapeDtypeStruct((HEADS, SEQS), jnp.float32),
         ),
         scratch_shapes=[
             pltpu.VMEM((ITEMS, DK, DV), jnp.float32),
@@ -248,11 +265,58 @@
             pltpu.SemaphoreType.DMA((CHUNKS,)),
         ],
         name="memory",
-    )(coef, k, ko, v, vo, norm, state)
+    )(coef, k, ko, v, norm, state)
+
+
+def copies_kernel(block_ref, out_ref):
+    for i in range(out_ref.shape[0]):
+        out_ref[i] = block_ref[...]
 
 
 def to_each(block, count):
-    return jnp.broadcast_to(block[None], (count, *block.shape))
+    return pl.pallas_call(
+        copies_kernel,
+        in_specs=[VMEM],
+        out_specs=VMEM,
+        out_shape=pltpu.VMEM((count, *block.shape), block.dtype),
+        name="to_each",
+    )(block)
+
+
+def join_kernel(terms_ref, out_ref, *, tps, block):
+    cross = terms_ref.shape[0] // tps
+    lane = iota((SEQS, DK), 1) // block
+    for part in range(terms_ref.shape[2] // DK):
+        cols = slice(part * DK, (part + 1) * DK)
+        sums = [
+            sum(terms_ref[g * tps + t, :, cols].astype(jnp.float32) for t in range(tps))
+            for g in range(cross)
+        ]
+        step = 1
+        while step < cross:
+            low = lane & step == 0
+            swapped = list(sums)
+            for g in range(cross):
+                if g & step == 0:
+                    a, b = sums[g], sums[g + step]
+                    swapped[g] = jnp.where(low, a, pltpu.roll(b, step * block, 1))
+                    swapped[g + step] = jnp.where(low, pltpu.roll(a, DK - step * block, 1), b)
+            sums = swapped
+            step *= 2
+        for z in range(cross):
+            at = (part * cross + z) * DK
+            out_ref[:, at : at + DK] = sums[z].astype(jnp.bfloat16)
+
+
+def joined(terms, tps, block):
+    sources, seqs, cols = terms.shape
+    return pl.pallas_call(
+        functools.partial(join_kernel, tps=tps, block=block),
+        in_specs=[VMEM],
+        out_specs=VMEM,
+        out_shape=jax.ShapeDtypeStruct((seqs, sources // tps * cols), jnp.bfloat16),
+        name="join",
+    )(terms)
 
 
 def exchanged(pieces, axes):
@@ -279,31 +343,35 @@
     zs, cross, tps = lax.axis_size("kv_0"), lax.axis_size(PLANE), lax.axis_size("tp")
     weight = exchanged(to_each(out_weight.T, zs), "kv_0")
     weight = weight.reshape(-1, out_weight.shape[0])
-    q, k, ko, v, vo = (
-        a.reshape(ROWS, -1) for a in (queries, keys, old_keys, values, old_values)
+    q, k, ko = (a.reshape(ROWS, DK) for a in (queries, keys, old_keys))
+    v, vo = (
+        a.reshape(SEQS, PROPS, HEADS, 2, DK).swapaxes(2, 3).reshape(RUN, DK)
+        for a in (values, old_values)
     )
     gates = (
         a.transpose(1, 2, 0) for a in (in_gate, forget_pre, old_in_gate, old_forget)
     )
     norm = state_norm.reshape(ITEMS, DK)
     state = state_mem.reshape(ITEMS, DK, DV)
-    hidden, coef = hidden_of(
+    hidden, coef, run_values = hidden_of(
         q, k, ko, v, vo, *gates, accepted[None], state_max.T, norm, norm_gain, state
     )
     rows = lax.all_gather(hidden.reshape(PROPS * SEQS, -1), PLANE, tiled=True)
-    new_mem, new_norm = memory_of(coef, k, ko, v, vo, norm, state)
     terms = lax.dot_general(
         rows, weight, (((1,), (1,)), ((), ())), preferred_element_type=jnp.float32
     ).astype(jnp.bfloat16)
     terms = exchanged(terms.reshape(cross * tps, SEQS, -1), (*PLANE, "tp"))
-    total = terms.astype(jnp.float32).reshape(cross, tps, SEQS, zs, -1).sum(axis=1)
-    mixed = total.astype(jnp.bfloat16).transpose(1, 2, 0, 3).reshape(SEQS, 1, -1)
-    new_max = coef[2, :ROWS].reshape(SEQS, PROPS, HEADS)[:, 0]
+    coef, run_values = (
+        pltpu.with_memory_space_constraint(a, pltpu.VMEM) for a in (coef, run_values)
+    )
+    new_mem, new_norm, new_max = memory_of(coef, k, ko, run_values, norm, state)
+    terms = pltpu.with_memory_space_constraint(terms, pltpu.VMEM)
+    mixed = joined(terms, tps, out_weight.shape[1])[:, None]
     return (
         mixed,
         new_mem.reshape(state_mem.shape),
         new_norm.reshape(state_norm.shape),
-        new_max,
+        new_max.T,
     )
 
 

time: 57 us -> 54.1 us (0.949)
  local copies, waits for them, and re-layouts: 7.48 us -> 0 us
  Pallas kernels: 8.59 us -> 10.8 us
  starting transfers between devices: 22.4 us -> 23.9 us
  waiting for transfers between devices: 1.82 us -> 3.32 us
    reshape x4 -> x0, local copies, waits for them, and re-layouts: 4.4 us -> none  [the longest x2 2.77 us: on_device(): a.reshape(ROWS, -1)]
    pallas_call x1 -> x3, Pallas kernels: 4.27 us -> 6.52 us  [the longest x1 4.23 us: memory_of(): pl.pallas_call(memory_kernel, in_specs=[VMEM] * 5 + [ANY], out_specs=(ANY...]
    all_to_all x2, starting transfers between devices: 22.4 us -> 23.9 us  [exchanged(): return lax.all_to_all(pieces, axes, split_axis=0, concat_axis=0, tiled=True)]
    all_to_all x2, waiting for transfers between devices: 1.82 us -> 3.32 us  [exchanged(): return lax.all_to_all(pieces, axes, split_axis=0, concat_axis=0, tiled=True)]
    broadcast_in_dim x1 -> x0, local copies, waits for them, and re-layouts: 1.45 us -> none  [to_each(): return jnp.broadcast_to(block[None], (count, *block.shape))]
    slice x3 -> x0, local copies, waits for them, and re-layouts: 1.35 us -> none  [on_device(): new_max = coef[2, :ROWS].reshape(SEQS, PROPS, HEADS)[:, 0]]
  transfers between devices with their start and end apart: 2 -> 2, of which waited for: 1 -> 1; matrix products, arithmetic and copies ran while one was open for 8% -> 0% of each run, Pallas kernels for 15% -> 16%
where the time goes in v2:
time: 54.1 us; the launch traced here: 53.6 us
  starting transfers between devices  23.9 us (44%)
  blocking collectives  14 us (26%)
  Pallas kernels  10.8 us (20%)
  waiting for transfers between devices  3.32 us (6%)
  matrix products  0.91 us (2%)
  between operations  0.66 us (1%)
    all_to_all x2, starting transfers between devices, exchanged(): return lax.all_to_all(pieces, axes, split_axis=0, concat_axis=0, tiled=True)  23.9 us
    all_gather x1, blocking collectives, on_device(): rows = lax.all_gather(hidden.reshape(PROPS * SEQS, -1), PLANE, tiled=True)  14 us
    pallas_call x1, Pallas kernels, hidden_of(): pl.pallas_call(hidden_kernel, in_specs=[VMEM] * 13 + [ANY], out_specs=(VM...  4.29 us
    pallas_call x1, Pallas kernels, memory_of(): pl.pallas_call(memory_kernel, in_specs=[VMEM] * 5 + [ANY], out_specs=(ANY...  4.23 us
    all_to_all x2, waiting for transfers between devices, exchanged(): return lax.all_to_all(pieces, axes, split_axis=0, concat_axis=0, tiled=True)  3.32 us
    pallas_call x1, Pallas kernels, to_each(): pl.pallas_call(copies_kernel, in_specs=[VMEM], out_specs=VMEM, out_shape=...  1.44 us
  transfers between devices with their start and end apart: 2, of which 1 were waited for; matrix products, arithmetic and copies ran while one was open for 0% of the time, Pallas kernels for 16%

profile of v2, /device:TPU:1, one launch (start us, length us, event | category | flops | bytes accessed | tf_op | source)
XLA Modules:
  0.0 53.6 jit_solution(11505739668347741227)
XLA Ops:
  0.6 1.4 %to_each.1 = bf16[16,16,512]{2,1,0:T(8,128)(2,1)} custom-call(bf16[16,512]{1,0:T(8,128)(2,1)} %bitcast.46), custom_call_target="tpu_custom_call" | custom-call | tf_op jit(solution)/shard_map/to_each/pallas_call | solution.py:277
  2.1 15.7 %all-to-all-start = ((bf16[16,16,512]{2,1,0:T(8,128)(2,1)}), bf16[16,16,512]{2,1,0:T(8,128)(2,1)S(1)}, u32[]{:S(2)}, u32[]{:S(2)}) async-start(bf16[16,16,512]{2,1,0:T(8,128)(2,1)} %to_each.1), calls=%async_computation | async-start | bytes 524288 | tf_op jit(solution)/shard_map/all_to_all | solution.py:323
  17.8 4.3 %hidden.1 = (bf16[4,8,512]{2,1,0:T(8,128)(2,1)S(1)}, f32[8,128]{1,0:T(8,128)S(1)}, bf16[128,256]{1,0:T(8,128)(2,1)S(1)}) custom-call(bf16[64,128]{1,0:T(8,128)(2,1)} %bitcast.45, bf16[64,128]{1,0:T(8,128)(2,1)} %bitcast.36, bf16[64,128]{1,0:T(8,128)(2,1)} %bitcast.38, bf16[128,128]{1,0:T(8,128)(2,1)} %bitcast.40, bf16[128,128]{1,0:T(8,128)(2,1)} %bitcast.41, ...), custom_call_target="tpu_custom_call" | custom-call | tf_op jit(solution)/shard_map/hidden/pallas_call | solution.py:233
  22.1 14.0 %all_gather.3 = bf16[256,512]{1,0:T(8,128)(2,1)S(1)} all-gather(bf16[32,512]{1,0:T(8,128)(2,1)S(1)} %bitcast.32), channel_id=1, replica_groups=mesh['kv_0'=16,'kv_1'=4,'kv_2'=2,'tp'=4] {'kv_1','kv_2'}, dimensions={0}, use_global_device_ids=true | all-gather | bytes 294912 | tf_op jit(solution)/shard_map/all_gather | solution.py:359
  36.1 0.0 all-to-all-done
  36.1 0.9 %fusion = bf16[32,8,256]{2,1,0:T(8,128)(2,1)} fusion(bf16[256,512]{1,0:T(8,128)(2,1)S(1)} %all_gather.3, bf16[256,512]{1,0:T(8,128)(2,1)S(1)} %bitcast.35), kind=kOutput, calls=%fused_computation.1 | convolution fusion | flops 67174400 | bytes 655360 | tf_op jit(solution)/shard_map/dot_general | solution.py:360
  37.0 8.1 %all-to-all-start.1 = ((bf16[32,8,256]{2,1,0:T(8,128)(2,1)}), bf16[32,8,256]{2,1,0:T(8,128)(2,1)S(1)}, u32[]{:S(2)}, u32[]{:S(2)}) async-start(bf16[32,8,256]{2,1,0:T(8,128)(2,1)} %fusion), calls=%async_computation.1 | async-start | bytes 262144 | tf_op jit(solution)/shard_map/all_to_all | solution.py:323
  45.1 4.2 %memory.1 = (f32[16,128,256]{2,1,0:T(8,128)}, f32[16,128]{1,0:T(8,128)}, f32[2,8]{1,0:T(2,128)}) custom-call(f32[8,128]{1,0:T(8,128)S(1)} %get-tuple-element.11.coef_ref, bf16[64,128]{1,0:T(8,128)(2,1)} %bitcast.37, bf16[64,128]{1,0:T(8,128)(2,1)} %bitcast.39, bf16[128,256]{1,0:T(8,128)(2,1)S(1)} %get-tuple-element.12.values_ref, f32[16,128]{1,0:T(8,128)} %bitcast.43, ...), custom_call_target="tpu_custom_call" | custom-call | tf_op jit(solution)/shard_map/memory/pallas_call | solution.py:252
  49.4 3.3 %all-to-all-done.1.terms_ref = bf16[32,8,256]{2,1,0:T(8,128)(2,1)S(1)} async-done(((bf16[32,8,256]{2,1,0:T(8,128)(2,1)}), bf16[32,8,256]{2,1,0:T(8,128)(2,1)S(1)}, u32[]{:S(2)}, u32[]{:S(2)}) %all-to-all-start.1) | async-done | bytes 131104 | tf_op jit(solution)/shard_map/all_to_all | solution.py:323
  52.7 0.8 %join.1 = bf16[8,2048]{1,0:T(8,128)(2,1)} custom-call(bf16[32,8,256]{2,1,0:T(8,128)(2,1)S(1)} %all-to-all-done.1.terms_ref), custom_call_target="tpu_custom_call" | custom-call | tf_op jit(solution)/shard_map/join/pallas_call | solution.py:313
Async XLA Ops:
  2.1 34.0 %all-to-all-start = ((bf16[16,16,512]{2,1,0:T(8,128)(2,1)}), bf16[16,16,512]{2,1,0:T(8,128)(2,1)S(1)}, u32[]{:S(2)}, u32[]{:S(2)}) async-start(bf16[16,16,512]{2,1,0:T(8,128)(2,1)} %to_each.1), calls=%async_computation | async-start | bytes 524288 | tf_op jit(solution)/shard_map/all_to_all | solution.py:323
  37.0 15.7 %all-to-all-start.1 = ((bf16[32,8,256]{2,1,0:T(8,128)(2,1)}), bf16[32,8,256]{2,1,0:T(8,128)(2,1)S(1)}, u32[]{:S(2)}, u32[]{:S(2)}) async-start(bf16[32,8,256]{2,1,0:T(8,128)(2,1)} %fusion), calls=%async_computation.1 | async-start | bytes 262144 | tf_op jit(solution)/shard_map/all_to_all | solution.py:323

commit v3 on v2

--- a/solution.py
+++ b/solution.py
@@ -9,7 +9,6 @@
 from jax.sharding import PartitionSpec as P
 
 KV = ("kv_0", "kv_1", "kv_2")
-PLANE = ("kv_1", "kv_2")
 
 SEQS = 8
 PROPS = 4
@@ -151,6 +150,8 @@
     inv = 1.0 / jnp.maximum(jnp.abs(den), 1.0)
     gain = jnp.where(iota((ROWS // CHUNKS, DV), 0) % 2 == 0, gain_ref[0:1, :], gain_ref[1:2, :])
 
+    for copy in copies:
+        copy.wait()
     size = ROWS // CHUNKS
     for c in range(CHUNKS):
         lo, hi = c * size, (c + 1) * size
@@ -159,7 +160,6 @@
         lhs = jnp.concatenate(
             [jnp.where(item == c * CHUNK + i, qc, 0.0) for i in range(CHUNK)], axis=1
         ).astype(jnp.bfloat16)
-        copies[c].wait()
         s_high, s_low = halves(state[pl.ds(c * CHUNK, CHUNK)].reshape(CHUNK * DK, DV))
         num = jnp.dot(lhs, s_high, preferred_element_type=jnp.float32) + jnp.dot(
             lhs, s_low, preferred_element_type=jnp.float32
@@ -226,6 +226,7 @@
 
 
 VMEM = pl.BlockSpec(memory_space=pltpu.VMEM)
+SMEM = pl.BlockSpec(memory_space=pltpu.SMEM)
 ANY = pl.BlockSpec(memory_space=pl.ANY)
 
 
@@ -283,15 +284,50 @@
     )(block)
 
 
-def join_kernel(terms_ref, out_ref, *, tps, block):
-    cross = terms_ref.shape[0] // tps
+def product_kernel(x_ref, *refs):
+    *row_refs, own_ref, swapped_ref, out_ref = refs
+    rows = jnp.concatenate([ref[...] for ref in row_refs], axis=0)
+    size = own_ref.shape[0]
+    for half, ref in enumerate((own_ref, swapped_ref)):
+        terms = dot_bt(rows, ref[...]).astype(jnp.bfloat16)
+        for d in range(len(row_refs)):
+            for p in range(PROPS):
+                at = (d * PROPS + p) * SEQS
+                out_ref[(x_ref[0] ^ d) * PROPS + p, :, half * size : (half + 1) * size] = terms[
+                    at : at + SEQS
+                ]
+
+
+def product(x, rows, own, swapped):
+    return pl.pallas_call(
+        product_kernel,
+        in_specs=[SMEM] + [VMEM] * (len(rows) + 2),
+        out_specs=VMEM,
+        out_shape=jax.ShapeDtypeStruct(
+            (len(rows) * PROPS, SEQS, 2 * own.shape[0]), jnp.bfloat16
+        ),
+        name="product",
+    )(x, *rows, own, swapped)
+
+
+def join_kernel(core_ref, terms_ref, out_ref, *, tps, block):
+    cross, size = terms_ref.shape[0] // tps * 2, terms_ref.shape[2] // 2
     lane = iota((SEQS, DK), 1) // block
-    for part in range(terms_ref.shape[2] // DK):
-        cols = slice(part * DK, (part + 1) * DK)
-        sums = [
-            sum(terms_ref[g * tps + t, :, cols].astype(jnp.float32) for t in range(tps))
-            for g in range(cross)
-        ]
+    swap = jnp.full((SEQS, DK), core_ref[0], jnp.int32) == 1
+    for part in range(size // DK):
+        sums = []
+        for g in range(cross // 2):
+            pair = []
+            for half in range(2):
+                at = half * size + part * DK
+                pair.append(
+                    sum(
+                        terms_ref[g * tps + t, :, at : at + DK].astype(jnp.float32)
+                        for t in range(tps)
+                    )
+                )
+            own, other = pair
+            sums += [jnp.where(swap, other, own), jnp.where(swap, own, other)]
         step = 1
         while step < cross:
             low = lane & step == 0
@@ -308,19 +344,27 @@
             out_ref[:, at : at + DK] = sums[z].astype(jnp.bfloat16)
 
 
-def joined(terms, tps, block):
+def joined(core, terms, tps, block):
     sources, seqs, cols = terms.shape
     return pl.pallas_call(
         functools.partial(join_kernel, tps=tps, block=block),
-        in_specs=[VMEM],
+        in_specs=[SMEM, VMEM],
         out_specs=VMEM,
         out_shape=jax.ShapeDtypeStruct((seqs, sources // tps * cols), jnp.bfloat16),
         name="join",
-    )(terms)
+    )(core, terms)
+
+
+def in_vmem(array):
+    return pltpu.with_memory_space_constraint(array, pltpu.VMEM)
 
 
 def exchanged(pieces, axes):
     return lax.all_to_all(pieces, axes, split_axis=0, concat_axis=0, tiled=True)
+
+
+def traded(block, axis, d):
+    return lax.ppermute(block, axis, [(i, i ^ d) for i in range(lax.axis_size(axis))])
 
 
 def on_device(
@@ -340,9 +384,9 @@
     norm_gain,
     out_weight,
 ):
-    zs, cross, tps = lax.axis_size("kv_0"), lax.axis_size(PLANE), lax.axis_size("tp")
-    weight = exchanged(to_each(out_weight.T, zs), "kv_0")
-    weight = weight.reshape(-1, out_weight.shape[0])
+    zs, xs, tps = lax.axis_size("kv_0"), lax.axis_size("kv_1"), lax.axis_size("tp")
+    own = exchanged(to_each(out_weight.T, zs), "kv_0")
+    own = own.reshape(-1, out_weight.shape[0])
     q, k, ko = (a.reshape(ROWS, DK) for a in (queries, keys, old_keys))
     v, vo = (
         a.reshape(SEQS, PROPS, HEADS, 2, DK).swapaxes(2, 3).reshape(RUN, DK)
@@ -356,17 +400,17 @@
     hidden, coef, run_values = hidden_of(
         q, k, ko, v, vo, *gates, accepted[None], state_max.T, norm, norm_gain, state
     )
-    rows = lax.all_gather(hidden.reshape(PROPS * SEQS, -1), PLANE, tiled=True)
-    terms = lax.dot_general(
-        rows, weight, (((1,), (1,)), ((), ())), preferred_element_type=jnp.float32
-    ).astype(jnp.bfloat16)
-    terms = exchanged(terms.reshape(cross * tps, SEQS, -1), (*PLANE, "tp"))
-    coef, run_values = (
-        pltpu.with_memory_space_constraint(a, pltpu.VMEM) for a in (coef, run_values)
-    )
-    new_mem, new_norm, new_max = memory_of(coef, k, ko, run_values, norm, state)
-    terms = pltpu.with_memory_space_constraint(terms, pltpu.VMEM)
-    mixed = joined(terms, tps, out_weight.shape[1])[:, None]
+    hidden = hidden.reshape(PROPS * SEQS, -1)
+    rows = [hidden]
+    for d in range(1, xs):
+        rows.append(traded(hidden, "kv_1", d))
+    swapped = traded(own, "kv_2", 1)
+    place = [lax.axis_index(a)[None].astype(jnp.int32) for a in ("kv_1", "kv_2")]
+    *rows, own, swapped = (in_vmem(a) for a in (*rows, own, swapped))
+    terms = product(place[0], rows, own, swapped)
+    terms = exchanged(terms, ("kv_1", "tp"))
+    new_mem, new_norm, new_max = memory_of(in_vmem(coef), k, ko, in_vmem(run_values), norm, state)
+    mixed = joined(place[1], in_vmem(terms), tps, out_weight.shape[1])[:, None]
     return (
         mixed,
         new_mem.reshape(state_mem.shape),

time: 54.1 us -> 70.1 us (1.30)
  the two profiles are of different devices: /device:TPU:1 before, /device:TPU:32 now
where the time goes in v3:
time: 70.1 us; the launch traced here: 69.5 us
  blocking collectives  32.9 us (47%)
  starting transfers between devices  18.5 us (26%)
  Pallas kernels  10.5 us (15%)
  waiting for transfers between devices  6.94 us (10%)
  between operations  0.71 us (1%)
    all_to_all x1, blocking collectives, exchanged(): return lax.all_to_all(pieces, axes, split_axis=0, concat_axis=0, tiled=True)  32.9 us
    ppermute x4, starting transfers between devices, traded(): lax.ppermute(block, axis, [(i, i ^ d) for i in range(lax.axis_size(axis))])  11.7 us
    all_to_all x1, starting transfers between devices, exchanged(): return lax.all_to_all(pieces, axes, split_axis=0, concat_axis=0, tiled=True)  6.74 us
    pallas_call x1, Pallas kernels, memory_of(): pl.pallas_call(memory_kernel, in_specs=[VMEM] * 5 + [ANY], out_specs=(ANY...  4.23 us
    pallas_call x1, Pallas kernels, hidden_of(): pl.pallas_call(hidden_kernel, in_specs=[VMEM] * 13 + [ANY], out_specs=(VM...  3.68 us
    all_to_all x1, waiting for transfers between devices, exchanged(): return lax.all_to_all(pieces, axes, split_axis=0, concat_axis=0, tiled=True)  3.6 us
    ppermute x4, waiting for transfers between devices, traded(): lax.ppermute(block, axis, [(i, i ^ d) for i in range(lax.axis_size(axis))])  3.35 us
  transfers between devices with their start and end apart: 5, of which 3 were waited for; matrix products, arithmetic and copies ran while one was open for 0% of the time, Pallas kernels for 11%

profile of v3, /device:TPU:32, one launch (start us, length us, event | category | flops | bytes accessed | tf_op | source)
XLA Modules:
  0.0 69.5 jit_solution(13341228422450084162)
XLA Ops:
  0.6 0.7 %to_each.1 = bf16[16,16,512]{2,1,0:T(8,128)(2,1)S(1)} custom-call(bf16[16,512]{1,0:T(8,128)(2,1)} %bitcast.48), custom_call_target="tpu_custom_call" | custom-call | tf_op jit(solution)/shard_map/to_each/pallas_call | solution.py:278
  1.4 32.9 %all_to_all.10 = bf16[16,16,512]{2,1,0:T(8,128)(2,1)S(1)} all-to-all(bf16[16,16,512]{2,1,0:T(8,128)(2,1)S(1)} %to_each.1), channel_id=1, replica_groups=mesh['kv_0'=16,'kv_1'=4,'kv_2'=2,'tp'=4] {'kv_0'}, dimensions={0} | all-to-all | bytes 524288 | tf_op jit(solution)/shard_map/all_to_all | solution.py:363
  34.3 1.9 %collective-permute-start.3 = (bf16[256,512]{1,0:T(8,128)(2,1)S(1)}, bf16[256,512]{1,0:T(8,128)(2,1)S(1)}, u32[]{:S(2)}, u32[]{:S(2)}) collective-permute-start(bf16[256,512]{1,0:T(8,128)(2,1)S(1)} %bitcast.30), channel_id=1, source_target_pairs={{0,4},{4,0},{1,5},{5,1},{2,6},{6,2},{3,7},{7,3},{8,12},{12,8},{9,1... | collective-permute-start | bytes 786440 | tf_op jit(solution)/shard_map/ppermute | solution.py:367
  36.2 3.7 %hidden.1 = (bf16[4,8,512]{2,1,0:T(8,128)(2,1)S(1)}, f32[8,128]{1,0:T(8,128)S(1)}, bf16[128,256]{1,0:T(8,128)(2,1)S(1)}) custom-call(bf16[64,128]{1,0:T(8,128)(2,1)} %bitcast.47, bf16[64,128]{1,0:T(8,128)(2,1)} %bitcast.38, bf16[64,128]{1,0:T(8,128)(2,1)} %bitcast.40, bf16[128,128]{1,0:T(8,128)(2,1)} %bitcast.42, bf16[128,128]{1,0:T(8,128)(2,1)} %bitcast.43, ...), custom_call_target="tpu_custom_call" | custom-call | tf_op jit(solution)/shard_map/hidden/pallas_call | solution.py:234
  39.9 4.7 %collective-permute-start.2 = (bf16[32,512]{1,0:T(8,128)(2,1)S(1)}, bf16[32,512]{1,0:T(8,128)(2,1)S(1)}, u32[]{:S(2)}, u32[]{:S(2)}) collective-permute-start(bf16[32,512]{1,0:T(8,128)(2,1)S(1)} %bitcast.32), channel_id=1, source_target_pairs={{0,24},{8,16},{16,8},{24,0},{1,25},{9,17},{17,9},{25,1},{2,26},{10... | collective-permute-start | bytes 98312 | tf_op jit(solution)/shard_map/ppermute | solution.py:367
  44.6 2.7 %collective-permute-start.1 = (bf16[32,512]{1,0:T(8,128)(2,1)S(1)}, bf16[32,512]{1,0:T(8,128)(2,1)S(1)}, u32[]{:S(2)}, u32[]{:S(2)}) collective-permute-start(bf16[32,512]{1,0:T(8,128)(2,1)S(1)} %bitcast.33), channel_id=1, source_target_pairs={{0,16},{8,24},{16,0},{24,8},{1,17},{9,25},{17,1},{25,9},{2,18},{10... | collective-permute-start | bytes 98312 | tf_op jit(solution)/shard_map/ppermute | solution.py:367
  47.3 2.4 %collective-permute-start = (bf16[32,512]{1,0:T(8,128)(2,1)S(1)}, bf16[32,512]{1,0:T(8,128)(2,1)S(1)}, u32[]{:S(2)}, u32[]{:S(2)}) collective-permute-start(bf16[32,512]{1,0:T(8,128)(2,1)S(1)} %bitcast.34), channel_id=1, source_target_pairs={{0,8},{8,0},{16,24},{24,16},{1,9},{9,1},{17,25},{25,17},{2,10},{10... | collective-permute-start | bytes 98312 | tf_op jit(solution)/shard_map/ppermute | solution.py:367
  49.7 0.0 collective-permute-done.2.refs_3_
  49.8 2.1 %collective-permute-done.1.refs_2_ = bf16[32,512]{1,0:T(8,128)(2,1)S(1)} collective-permute-done((bf16[32,512]{1,0:T(8,128)(2,1)S(1)}, bf16[32,512]{1,0:T(8,128)(2,1)S(1)}, u32[]{:S(2)}, u32[]{:S(2)}) %collective-permute-start.1) | collective-permute-done | bytes 32800 | tf_op jit(solution)/shard_map/ppermute | solution.py:367
  51.9 1.2 %collective-permute-done.refs_1_ = bf16[32,512]{1,0:T(8,128)(2,1)S(1)} collective-permute-done((bf16[32,512]{1,0:T(8,128)(2,1)S(1)}, bf16[32,512]{1,0:T(8,128)(2,1)S(1)}, u32[]{:S(2)}, u32[]{:S(2)}) %collective-permute-start) | collective-permute-done | bytes 32800 | tf_op jit(solution)/shard_map/ppermute | solution.py:367
  53.1 0.0 collective-permute-done.3.refs_5_
  53.1 1.0 %product.1 = bf16[16,8,512]{2,1,0:T(8,128)(2,1)} custom-call(s32[1]{0:T(128)} %bitcast.1.x_ref, bf16[32,512]{1,0:T(8,128)(2,1)S(1)} %bitcast.35, bf16[32,512]{1,0:T(8,128)(2,1)S(1)} %collective-permute-done.refs_1_, bf16[32,512]{1,0:T(8,128)(2,1)S(1)} %collective-permute-done.1.refs_2_, bf16[32,512]{1,0:T(8,128)(2,1)S(1)} %collective-permute-done.2.refs_3_, ...), custom_call_target="tpu_custom_call" | custom-call | tf_op jit(solution)/shard_map/product/pallas_call | solution.py:302
  54.1 6.7 %all-to-all-start.1 = ((bf16[16,8,512]{2,1,0:T(8,128)(2,1)}), bf16[16,8,512]{2,1,0:T(8,128)(2,1)S(1)}, u32[]{:S(2)}, u32[]{:S(2)}) async-start(bf16[16,8,512]{2,1,0:T(8,128)(2,1)} %product.1), calls=%async_computation.1 | async-start | bytes 262144 | tf_op jit(solution)/shard_map/all_to_all | solution.py:363
  60.8 4.2 %memory.1 = (f32[16,128,256]{2,1,0:T(8,128)}, f32[16,128]{1,0:T(8,128)}, f32[2,8]{1,0:T(2,128)}) custom-call(f32[8,128]{1,0:T(8,128)S(1)} %get-tuple-element.11.coef_ref, bf16[64,128]{1,0:T(8,128)(2,1)} %bitcast.39, bf16[64,128]{1,0:T(8,128)(2,1)} %bitcast.41, bf16[128,256]{1,0:T(8,128)(2,1)S(1)} %get-tuple-element.12.values_ref, f32[16,128]{1,0:T(8,128)} %bitcast.45, ...), custom_call_target="tpu_custom_call" | custom-call | tf_op jit(solution)/shard_map/memory/pallas_call | solution.py:253
  65.1 3.6 %all-to-all-done.1.terms_ref = bf16[16,8,512]{2,1,0:T(8,128)(2,1)S(1)} async-done(((bf16[16,8,512]{2,1,0:T(8,128)(2,1)}), bf16[16,8,512]{2,1,0:T(8,128)(2,1)S(1)}, u32[]{:S(2)}, u32[]{:S(2)}) %all-to-all-start.1) | async-done | bytes 131104 | tf_op jit(solution)/shard_map/all_to_all | solution.py:363
  68.7 0.8 %join.1 = bf16[8,2048]{1,0:T(8,128)(2,1)} custom-call(s32[1]{0:T(128)} %bitcast.core_ref, bf16[16,8,512]{2,1,0:T(8,128)(2,1)S(1)} %all-to-all-done.1.terms_ref), custom_call_target="tpu_custom_call" | custom-call | tf_op jit(solution)/shard_map/join/pallas_call | solution.py:349
Async XLA Ops:
  34.3 18.8 %collective-permute-start.3 = (bf16[256,512]{1,0:T(8,128)(2,1)S(1)}, bf16[256,512]{1,0:T(8,128)(2,1)S(1)}, u32[]{:S(2)}, u32[]{:S(2)}) collective-permute-start(bf16[256,512]{1,0:T(8,128)(2,1)S(1)} %bitcast.30), channel_id=1, source_target_pairs={{0,4},{4,0},{1,5},{5,1},{2,6},{6,2},{3,7},{7,3},{8,12},{12,8},{9,1... | collective-permute-start | bytes 786440 | tf_op jit(solution)/shard_map/ppermute | solution.py:367
  39.9 9.9 %collective-permute-start.2 = (bf16[32,512]{1,0:T(8,128)(2,1)S(1)}, bf16[32,512]{1,0:T(8,128)(2,1)S(1)}, u32[]{:S(2)}, u32[]{:S(2)}) collective-permute-start(bf16[32,512]{1,0:T(8,128)(2,1)S(1)} %bitcast.32), channel_id=1, source_target_pairs={{0,24},{8,16},{16,8},{24,0},{1,25},{9,17},{17,9},{25,1},{2,26},{10... | collective-permute-start | bytes 98312 | tf_op jit(solution)/shard_map/ppermute | solution.py:367
  44.6 7.3 %collective-permute-start.1 = (bf16[32,512]{1,0:T(8,128)(2,1)S(1)}, bf16[32,512]{1,0:T(8,128)(2,1)S(1)}, u32[]{:S(2)}, u32[]{:S(2)}) collective-permute-start(bf16[32,512]{1,0:T(8,128)(2,1)S(1)} %bitcast.33), channel_id=1, source_target_pairs={{0,16},{8,24},{16,0},{24,8},{1,17},{9,25},{17,1},{25,9},{2,18},{10... | collective-permute-start | bytes 98312 | tf_op jit(solution)/shard_map/ppermute | solution.py:367
  47.3 5.8 %collective-permute-start = (bf16[32,512]{1,0:T(8,128)(2,1)S(1)}, bf16[32,512]{1,0:T(8,128)(2,1)S(1)}, u32[]{:S(2)}, u32[]{:S(2)}) collective-permute-start(bf16[32,512]{1,0:T(8,128)(2,1)S(1)} %bitcast.34), channel_id=1, source_target_pairs={{0,8},{8,0},{16,24},{24,16},{1,9},{9,1},{17,25},{25,17},{2,10},{10... | collective-permute-start | bytes 98312 | tf_op jit(solution)/shard_map/ppermute | solution.py:367
  54.1 14.6 %all-to-all-start.1 = ((bf16[16,8,512]{2,1,0:T(8,128)(2,1)}), bf16[16,8,512]{2,1,0:T(8,128)(2,1)S(1)}, u32[]{:S(2)}, u32[]{:S(2)}) async-start(bf16[16,8,512]{2,1,0:T(8,128)(2,1)} %product.1), calls=%async_computation.1 | async-start | bytes 262144 | tf_op jit(solution)/shard_map/all_to_all | solution.py:363

commit v4 on v2

--- a/solution.py
+++ b/solution.py
@@ -21,7 +21,9 @@
 ITEMS = SEQS * HEADS
 CHUNK = 4
 CHUNKS = ITEMS // CHUNK
+KEPT = 8
 EPS = 1e-5
+FIRST_Z, FIRST_CROSS, FIRST_TP = 0, 5, 2
 
 
 def iota(shape, dim):
@@ -61,20 +63,20 @@
     return jnp.concatenate([rows[:ROWS], rows[ROWS:]], axis=1).astype(jnp.bfloat16)
 
 
-def state_copies(state_hbm, state, sems):
+def state_copies(state_hbm, rest, sems):
     return [
         pltpu.make_async_copy(
-            state_hbm.at[pl.ds(c * CHUNK, CHUNK)], state.at[pl.ds(c * CHUNK, CHUNK)], sems.at[c]
+            state_hbm.at[pl.ds(at, CHUNK)], rest.at[pl.ds(at - KEPT, CHUNK)], sems.at[i]
         )
-        for c in range(CHUNKS)
+        for i, at in enumerate(range(KEPT, ITEMS, CHUNK))
     ]
 
 
 def hidden_kernel(
     q_ref, k_ref, ko_ref, v_ref, vo_ref, ig_ref, fg_ref, igo_ref, fgo_ref, acc_ref, smax_ref,
-    norm_ref, gain_ref, state_hbm, hidden_ref, coef_ref, values_ref, state, flat, sems,
+    norm_ref, gain_ref, kept, state_hbm, hidden_ref, coef_ref, values_ref, rest, flat, sems,
 ):
-    copies = state_copies(state_hbm, state, sems)
+    copies = state_copies(state_hbm, rest, sems)
     for copy in copies:
         copy.start()
 
@@ -151,6 +153,8 @@
     inv = 1.0 / jnp.maximum(jnp.abs(den), 1.0)
     gain = jnp.where(iota((ROWS // CHUNKS, DV), 0) % 2 == 0, gain_ref[0:1, :], gain_ref[1:2, :])
 
+    for copy in copies:
+        copy.wait()
     size = ROWS // CHUNKS
     for c in range(CHUNKS):
         lo, hi = c * size, (c + 1) * size
@@ -159,8 +163,9 @@
         lhs = jnp.concatenate(
             [jnp.where(item == c * CHUNK + i, qc, 0.0) for i in range(CHUNK)], axis=1
         ).astype(jnp.bfloat16)
-        copies[c].wait()
-        s_high, s_low = halves(state[pl.ds(c * CHUNK, CHUNK)].reshape(CHUNK * DK, DV))
+        at = c * CHUNK
+        part = kept[pl.ds(at, CHUNK)] if at < KEPT else rest[pl.ds(at - KEPT, CHUNK)]
+        s_high, s_low = halves(part.reshape(CHUNK * DK, DV))
         num = jnp.dot(lhs, s_high, preferred_element_type=jnp.float32) + jnp.dot(
             lhs, s_low, preferred_element_type=jnp.float32
         )
@@ -179,10 +184,10 @@
 
 
 def memory_kernel(
-    coef_ref, k_ref, ko_ref, values_ref, norm_ref, state_hbm,
-    new_hbm, new_norm_ref, new_max_ref, state, new, sems, out_sems,
+    coef_ref, k_ref, ko_ref, values_ref, norm_ref, kept, state_hbm,
+    new_hbm, new_norm_ref, new_max_ref, rest, new, sems, out_sems,
 ):
-    copies = state_copies(state_hbm, state, sems)
+    copies = state_copies(state_hbm, rest, sems)
     for copy in copies:
         copy.start()
     tok, keep = coef_ref[0:1, :], coef_ref[1:2, :]
@@ -196,25 +201,26 @@
     mine = item_of(lane) == iota((ITEMS, RUN), 0)
     t_high, t_low = halves(jnp.where(mine, tok, 0.0))
     kb = k.astype(jnp.bfloat16)
-    kept = jnp.sum(jnp.where(mine & (place_of(lane) == 0), keep, 0.0), axis=1, keepdims=True)
+    share = jnp.sum(jnp.where(mine & (place_of(lane) == 0), keep, 0.0), axis=1, keepdims=True)
     new_norm_ref[...] = (
-        kept * norm_ref[...]
+        share * norm_ref[...]
         + jnp.dot(t_high, kb, preferred_element_type=jnp.float32)
         + jnp.dot(t_low, kb, preferred_element_type=jnp.float32)
     )
-    weighted = k.T * tok
+    high, low = halves(k.T * tok)
+    both = jnp.concatenate([high, low], axis=1)
     twice = jnp.concatenate([v, v], axis=0)
-    lane = item_of(iota((DK, RUN), 1))
+    lane = item_of(iota((8, 2 * RUN), 1) % RUN)
     stores = []
     for c in range(CHUNKS):
-        copies[c].wait()
+        if c * CHUNK >= KEPT:
+            copies[c - KEPT // CHUNK].wait()
         for i in range(c * CHUNK, (c + 1) * CHUNK):
-            high, low = halves(jnp.where(lane == i, weighted, 0.0))
-            update = jnp.dot(
-                jnp.concatenate([high, low], axis=1), twice, preferred_element_type=jnp.float32
-            )
+            mask = (lane == i).astype(jnp.float32)[:1].astype(jnp.bfloat16)
+            update = jnp.dot(both * mask, twice, preferred_element_type=jnp.float32)
             at = i // 2 * 8 + i % 2
-            new[i] = keep[:, at : at + 1] * state[i] + update
+            old = kept[i] if i < KEPT else rest[i - KEPT]
+            new[i] = keep[:, at : at + 1] * old + update
         stores.append(
             pltpu.make_async_copy(
                 new.at[pl.ds(c * CHUNK, CHUNK)], new_hbm.at[pl.ds(c * CHUNK, CHUNK)], out_sems.at[c]
@@ -229,10 +235,10 @@
 ANY = pl.BlockSpec(memory_space=pl.ANY)
 
 
-def hidden_of(q, k, ko, v, vo, ig, fg, igo, fgo, accepted, smax, norm, gain, state):
+def hidden_of(q, k, ko, v, vo, ig, fg, igo, fgo, accepted, smax, norm, gain, kept, state):
     return pl.pallas_call(
         hidden_kernel,
-        in_specs=[VMEM] * 13 + [ANY],
+        in_specs=[VMEM] * 14 + [ANY],
         out_specs=(VMEM, VMEM, VMEM),
         out_shape=(
             pltpu.VMEM((PROPS, SEQS, HEADS * DV), jnp.bfloat16),
@@ -240,18 +246,18 @@
             pltpu.VMEM((RUN, DV), jnp.bfloat16),
         ),
         scratch_shapes=[
-            pltpu.VMEM((ITEMS, DK, DV), jnp.float32),
+            pltpu.VMEM((ITEMS - KEPT, DK, DV), jnp.float32),
             pltpu.VMEM((2, ROWS, DK), jnp.float32),
             pltpu.SemaphoreType.DMA((CHUNKS,)),
         ],
         name="hidden",
-    )(q, k, ko, v, vo, ig, fg, igo, fgo, accepted, smax, norm, gain, state)
-
-
-def memory_of(coef, k, ko, v, norm, state):
+    )(q, k, ko, v, vo, ig, fg, igo, fgo, accepted, smax, norm, gain, kept, state)
+
+
+def memory_of(coef, k, ko, v, norm, kept, state):
     return pl.pallas_call(
         memory_kernel,
-        in_specs=[VMEM] * 5 + [ANY],
+        in_specs=[VMEM] * 6 + [ANY],
         out_specs=(ANY, VMEM, VMEM),
         out_shape=(
             jax.ShapeDtypeStruct((ITEMS, DK, DV), jnp.float32),
@@ -259,37 +265,80 @@
             jax.ShapeDtypeStruct((HEADS, SEQS), jnp.float32),
         ),
         scratch_shapes=[
-            pltpu.VMEM((ITEMS, DK, DV), jnp.float32),
+            pltpu.VMEM((ITEMS - KEPT, DK, DV), jnp.float32),
             pltpu.VMEM((ITEMS, DK, DV), jnp.float32),
             pltpu.SemaphoreType.DMA((CHUNKS,)),
             pltpu.SemaphoreType.DMA((CHUNKS,)),
         ],
         name="memory",
-    )(coef, k, ko, v, norm, state)
-
-
-def copies_kernel(block_ref, out_ref):
-    for i in range(out_ref.shape[0]):
-        out_ref[i] = block_ref[...]
-
-
-def to_each(block, count):
+    )(coef, k, ko, v, norm, kept, state)
+
+
+def front_kernel(block_hbm, *refs):
+    count = (len(refs) - 4) // 2
+    inputs, pieces_hbm, outputs = refs[:count], refs[count], refs[count + 1 : 2 * count + 1]
+    block, pieces, sems = refs[2 * count + 1 :]
+    first = pltpu.make_async_copy(block_hbm, block, sems.at[0])
+    first.start()
+    copies = [
+        pltpu.make_async_copy(src.at[pl.ds(0, dst.shape[0])], dst, sems.at[i + 2])
+        for i, (src, dst) in enumerate(zip(inputs, outputs, strict=True))
+    ]
+    for copy in copies:
+        copy.start()
+    first.wait()
+    for i in range(pieces.shape[0]):
+        pieces[i] = block[...]
+    last = pltpu.make_async_copy(pieces, pieces_hbm, sems.at[1])
+    last.start()
+    for copy in copies:
+        copy.wait()
+    last.wait()
+
+
+def front(block, count, arrays, state):
+    shape = (count, *block.shape)
+    outs = [pltpu.VMEM(a.shape, a.dtype) for a in arrays]
+    outs.append(pltpu.VMEM((KEPT, *state.shape[1:]), state.dtype))
     return pl.pallas_call(
-        copies_kernel,
-        in_specs=[VMEM],
+        front_kernel,
+        in_specs=[ANY] * (1 + len(outs)),
+        out_specs=[ANY] + [VMEM] * len(outs),
+        out_shape=[jax.ShapeDtypeStruct(shape, block.dtype), *outs],
+        scratch_shapes=[
+            pltpu.VMEM(block.shape, block.dtype),
+            pltpu.VMEM(shape, block.dtype),
+            pltpu.SemaphoreType.DMA((2 + len(outs),)),
+        ],
+        name="front",
+    )(block, *arrays, state)
+
+
+def product_kernel(rows_ref, weight_ref, out_ref, *, order):
+    terms = dot_bt(rows_ref[...], weight_ref[...]).astype(jnp.bfloat16)
+    for i, source in enumerate(order):
+        out_ref[i] = terms[source * SEQS : (source + 1) * SEQS]
+
+
+def product(rows, weight, order):
+    return pl.pallas_call(
+        functools.partial(product_kernel, order=order),
+        in_specs=[VMEM, VMEM],
         out_specs=VMEM,
-        out_shape=pltpu.VMEM((count, *block.shape), block.dtype),
-        name="to_each",
-    )(block)
-
-
-def join_kernel(terms_ref, out_ref, *, tps, block):
-    cross = terms_ref.shape[0] // tps
+        out_shape=pltpu.VMEM((len(order), SEQS, weight.shape[0]), jnp.bfloat16),
+        name="product",
+    )(rows, weight)
+
+
+def join_kernel(terms_ref, out_ref, *, order, tps, block):
+    cross = len(order) // tps
+    slot = {source: i for i, source in enumerate(order)}
+    planes = out_ref.shape[1] // DK
     lane = iota((SEQS, DK), 1) // block
     for part in range(terms_ref.shape[2] // DK):
         cols = slice(part * DK, (part + 1) * DK)
         sums = [
-            sum(terms_ref[g * tps + t, :, cols].astype(jnp.float32) for t in range(tps))
+            sum(terms_ref[slot[g * tps + t], :, cols].astype(jnp.float32) for t in range(tps))
             for g in range(cross)
         ]
         step = 1
@@ -304,14 +353,14 @@
             sums = swapped
             step *= 2
         for z in range(cross):
-            at = (part * cross + z) * DK
+            at = (FIRST_Z + part * cross + z) % planes * DK
             out_ref[:, at : at + DK] = sums[z].astype(jnp.bfloat16)
 
 
-def joined(terms, tps, block):
+def joined(terms, order, tps, block):
     sources, seqs, cols = terms.shape
     return pl.pallas_call(
-        functools.partial(join_kernel, tps=tps, block=block),
+        functools.partial(join_kernel, order=order, tps=tps, block=block),
         in_specs=[VMEM],
         out_specs=VMEM,
         out_shape=jax.ShapeDtypeStruct((seqs, sources // tps * cols), jnp.bfloat16),
@@ -319,8 +368,18 @@
     )(terms)
 
 
-def exchanged(pieces, axes):
-    return lax.all_to_all(pieces, axes, split_axis=0, concat_axis=0, tiled=True)
+def exchanged(pieces, axes, order):
+    return lax.all_to_all(
+        pieces, axes, split_axis=0, concat_axis=0, tiled=True, axis_index_groups=[order]
+    )
+
+
+def from_place(first, size):
+    return [(first + i) % size for i in range(size)]
+
+
+def in_vmem(array):
+    return pltpu.with_memory_space_constraint(array, pltpu.VMEM)
 
 
 def on_device(
@@ -341,8 +400,6 @@
     out_weight,
 ):
     zs, cross, tps = lax.axis_size("kv_0"), lax.axis_size(PLANE), lax.axis_size("tp")
-    weight = exchanged(to_each(out_weight.T, zs), "kv_0")
-    weight = weight.reshape(-1, out_weight.shape[0])
     q, k, ko = (a.reshape(ROWS, DK) for a in (queries, keys, old_keys))
     v, vo = (
         a.reshape(SEQS, PROPS, HEADS, 2, DK).swapaxes(2, 3).reshape(RUN, DK)
@@ -353,20 +410,21 @@
     )
     norm = state_norm.reshape(ITEMS, DK)
     state = state_mem.reshape(ITEMS, DK, DV)
-    hidden, coef, run_values = hidden_of(
-        q, k, ko, v, vo, *gates, accepted[None], state_max.T, norm, norm_gain, state
-    )
+    inputs = (q, k, ko, v, vo, *gates, accepted[None], state_max.T, norm, norm_gain)
+    pieces, *inputs = front(out_weight.T, zs, inputs, state)
+    inputs = [in_vmem(a) for a in inputs]
+    q, k, ko, *_, norm, _, kept = inputs
+    weight = exchanged(pieces, "kv_0", from_place(FIRST_Z, zs))
+    weight = weight.reshape(-1, out_weight.shape[0])
+    hidden, coef, run_values = hidden_of(*inputs, state)
     rows = lax.all_gather(hidden.reshape(PROPS * SEQS, -1), PLANE, tiled=True)
-    terms = lax.dot_general(
-        rows, weight, (((1,), (1,)), ((), ())), preferred_element_type=jnp.float32
-    ).astype(jnp.bfloat16)
-    terms = exchanged(terms.reshape(cross * tps, SEQS, -1), (*PLANE, "tp"))
-    coef, run_values = (
-        pltpu.with_memory_space_constraint(a, pltpu.VMEM) for a in (coef, run_values)
-    )
-    new_mem, new_norm, new_max = memory_of(coef, k, ko, run_values, norm, state)
-    terms = pltpu.with_memory_space_constraint(terms, pltpu.VMEM)
-    mixed = joined(terms, tps, out_weight.shape[1])[:, None]
+    order = [g * tps + t for g in from_place(FIRST_CROSS, cross) for t in from_place(FIRST_TP, tps)]
+    terms = product(in_vmem(rows), in_vmem(weight), order)
+    terms = exchanged(terms, (*PLANE, "tp"), order)
+    new_mem, new_norm, new_max = memory_of(
+        in_vmem(coef), k, ko, in_vmem(run_values), norm, kept, state
+    )
+    mixed = joined(in_vmem(terms), order, tps, out_weight.shape[1])[:, None]
     return (
         mixed,
         new_mem.reshape(state_mem.shape),

time: 54.1 us -> 51.5 us (0.952)
  starting transfers between devices: 23.9 us -> 27.3 us
  waiting for transfers between devices: 3.32 us -> 0.01 us
  Pallas kernels: 10.8 us -> 9.11 us
  matrix products: 0.91 us -> 0 us
    all_to_all x2, starting transfers between devices: 23.9 us -> 27.3 us  [exchanged(): lax.all_to_all(pieces, axes, split_axis=0, concat_axis=0, tiled=True, axi...]
    all_to_all x2, waiting for transfers between devices: 3.32 us -> 0.01 us  [exchanged(): lax.all_to_all(pieces, axes, split_axis=0, concat_axis=0, tiled=True, axi...]
    pallas_call x4 -> x5, Pallas kernels: 10.8 us -> 9.11 us  [the longest x1 3.62 us: memory_of(): pl.pallas_call(memory_kernel, in_specs=[VMEM] * 6 + [ANY], out_specs=(ANY...]
    dot_general x1 -> x0, matrix products: 0.91 us -> none  [on_device(): lax.dot_general(rows, weight, (((1,), (1,)), ((), ())), preferred_element...]
  transfers between devices with their start and end apart: 2 -> 2, of which waited for: 1 -> 0; matrix products, arithmetic and copies ran while one was open for 0% -> 0% of each run, Pallas kernels for 16% -> 11%
where the time goes in v4:
time: 51.5 us; the launch traced here: 51.1 us
  starting transfers between devices  27.3 us (53%)
  blocking collectives  14 us (27%)
  Pallas kernels  9.11 us (18%)
  between operations  0.69 us (1%)
    all_to_all x2, starting transfers between devices, exchanged(): lax.all_to_all(pieces, axes, split_axis=0, concat_axis=0, tiled=True, axi...  27.3 us
    all_gather x1, blocking collectives, on_device(): rows = lax.all_gather(hidden.reshape(PROPS * SEQS, -1), PLANE, tiled=True)  14 us
    pallas_call x1, Pallas kernels, memory_of(): pl.pallas_call(memory_kernel, in_specs=[VMEM] * 6 + [ANY], out_specs=(ANY...  3.62 us
    pallas_call x1, Pallas kernels, hidden_of(): pl.pallas_call(hidden_kernel, in_specs=[VMEM] * 14 + [ANY], out_specs=(VM...  2.13 us
    pallas_call x1, Pallas kernels, front(): pl.pallas_call(front_kernel, in_specs=[ANY] * (1 + len(outs)), out_specs=...  1.6 us
  transfers between devices with their start and end apart: 2, of which 0 were waited for; matrix products, arithmetic and copies ran while one was open for 0% of the time, Pallas kernels for 11%

profile of v4, /device:TPU:1, one launch (start us, length us, event | category | flops | bytes accessed | tf_op | source)
XLA Modules:
  0.0 51.1 jit_solution(9192736666274097985)
XLA Ops:
  0.6 1.6 %front.1 = (bf16[16,16,512]{2,1,0:T(8,128)(2,1)}, bf16[64,128]{1,0:T(8,128)(2,1)S(1)}, bf16[64,128]{1,0:T(8,128)(2,1)S(1)}, bf16[64,128]{1,0:T(8,128)(2,1)S(1)},...) custom-call(bf16[16,512]{1,0:T(8,128)(2,1)} %bitcast.36, ...), custom_call_target="tpu_custom_call" | custom-call | tf_op jit(solution)/shard_map/front/pallas_call | solution.py:303
  2.2 15.7 %all-to-all-start = ((bf16[16,16,512]{2,1,0:T(8,128)(2,1)}), bf16[16,16,512]{2,1,0:T(8,128)(2,1)S(1)}, u32[]{:S(2)}, u32[]{:S(2)}) async-start(bf16[16,16,512]{2,1,0:T(8,128)(2,1)} %get-tuple-element.40), calls=%async_computation | async-start | bytes 524288 | tf_op jit(solution)/shard_map/all_to_all | solution.py:372
  18.0 2.1 %hidden.1 = (bf16[4,8,512]{2,1,0:T(8,128)(2,1)S(1)}, f32[8,128]{1,0:T(8,128)S(1)}, bf16[128,256]{1,0:T(8,128)(2,1)S(1)}) custom-call(bf16[64,128]{1,0:T(8,128)(2,1)S(1)} %get-tuple-element.25.q_ref, bf16[64,128]{1,0:T(8,128)(2,1)S(1)} %get-tuple-element.26.k_ref, bf16[64,128]{1,0:T(8,128)(2,1)S(1)} %get-tuple-element.27.ko_ref, ...), custom_call_target="tpu_custom_call" | custom-call | tf_op jit(solution)/shard_map/hidden/pallas_call | solution.py:239
  20.1 14.0 %all_gather.3.rows_ref = bf16[256,512]{1,0:T(8,128)(2,1)S(1)} all-gather(bf16[32,512]{1,0:T(8,128)(2,1)S(1)} %bitcast.29), channel_id=1, replica_groups=mesh['kv_0'=16,'kv_1'=4,'kv_2'=2,'tp'=4] {'kv_1','kv_2'}, dimensions={0}, use_global_device_ids=true | all-gather | bytes 294912 | tf_op jit(solution)/shard_map/all_gather | solution.py:420
  34.1 0.0 all-to-all-done
  34.1 0.9 %product.1 = bf16[32,8,256]{2,1,0:T(8,128)(2,1)} custom-call(bf16[256,512]{1,0:T(8,128)(2,1)S(1)} %all_gather.3.rows_ref, bf16[256,512]{1,0:T(8,128)(2,1)S(1)} %bitcast.28), custom_call_target="tpu_custom_call" | custom-call | tf_op jit(solution)/shard_map/product/pallas_call | solution.py:324
  35.0 11.6 %all-to-all-start.1 = ((bf16[32,8,256]{2,1,0:T(8,128)(2,1)}), bf16[32,8,256]{2,1,0:T(8,128)(2,1)S(1)}, u32[]{:S(2)}, u32[]{:S(2)}) async-start(bf16[32,8,256]{2,1,0:T(8,128)(2,1)} %product.1), calls=%async_computation.1 | async-start | bytes 262144 | tf_op jit(solution)/shard_map/all_to_all | solution.py:372
  46.6 3.6 %memory.1 = (f32[16,128,256]{2,1,0:T(8,128)}, f32[16,128]{1,0:T(8,128)}, f32[2,8]{1,0:T(2,128)}) custom-call(f32[8,128]{1,0:T(8,128)S(1)} %get-tuple-element.41.coef_ref, bf16[64,128]{1,0:T(8,128)(2,1)S(1)} %get-tuple-element.26.k_ref, bf16[64,128]{1,0:T(8,128)(2,1)S(1)} %get-tuple-element.27.ko_ref, bf16[128,256]{1,0:T(8,128)(2,1)S(1)} %get-tuple-element.42.values_ref, ...), custom_call_target="tpu_custom_call" | custom-call | tf_op jit(solution)/shard_map/memory/pallas_call | solution.py:258
  50.2 0.0 all-to-all-done.1.terms_ref
  50.2 0.8 %join.1 = bf16[8,2048]{1,0:T(8,128)(2,1)} custom-call(bf16[32,8,256]{2,1,0:T(8,128)(2,1)S(1)} %all-to-all-done.1.terms_ref), custom_call_target="tpu_custom_call" | custom-call | tf_op jit(solution)/shard_map/join/pallas_call | solution.py:362
Async XLA Ops:
  2.2 31.9 %all-to-all-start = ((bf16[16,16,512]{2,1,0:T(8,128)(2,1)}), bf16[16,16,512]{2,1,0:T(8,128)(2,1)S(1)}, u32[]{:S(2)}, u32[]{:S(2)}) async-start(bf16[16,16,512]{2,1,0:T(8,128)(2,1)} %get-tuple-element.40), calls=%async_computation | async-start | bytes 524288 | tf_op jit(solution)/shard_map/all_to_all | solution.py:372
  35.0 15.2 %all-to-all-start.1 = ((bf16[32,8,256]{2,1,0:T(8,128)(2,1)}), bf16[32,8,256]{2,1,0:T(8,128)(2,1)S(1)}, u32[]{:S(2)}, u32[]{:S(2)}) async-start(bf16[32,8,256]{2,1,0:T(8,128)(2,1)} %product.1), calls=%async_computation.1 | async-start | bytes 262144 | tf_op jit(solution)/shard_map/all_to_all | solution.py:372

commit v5 on v4

--- a/solution.py
+++ b/solution.py
@@ -21,9 +21,9 @@
 ITEMS = SEQS * HEADS
 CHUNK = 4
 CHUNKS = ITEMS // CHUNK
-KEPT = 8
+KEPT = 16
 EPS = 1e-5
-FIRST_Z, FIRST_CROSS, FIRST_TP = 0, 5, 2
+FIRST_Z, FIRST_CROSS, FIRST_TP = 12, 5, 2
 
 
 def iota(shape, dim):
@@ -66,16 +66,18 @@
 def state_copies(state_hbm, rest, sems):
     return [
         pltpu.make_async_copy(
-            state_hbm.at[pl.ds(at, CHUNK)], rest.at[pl.ds(at - KEPT, CHUNK)], sems.at[i]
-        )
-        for i, at in enumerate(range(KEPT, ITEMS, CHUNK))
+            state_hbm.at[pl.ds(KEPT + i * CHUNK, CHUNK)], part, sems.at[i]
+        )
+        for i, part in enumerate(rest)
     ]
 
 
 def hidden_kernel(
     q_ref, k_ref, ko_ref, v_ref, vo_ref, ig_ref, fg_ref, igo_ref, fgo_ref, acc_ref, smax_ref,
-    norm_ref, gain_ref, kept, state_hbm, hidden_ref, coef_ref, values_ref, rest, flat, sems,
+    norm_ref, gain_ref, *refs,
 ):
+    kept = refs[: KEPT // CHUNK]
+    state_hbm, hidden_ref, coef_ref, values_ref, *rest, flat, sems = refs[KEPT // CHUNK :]
     copies = state_copies(state_hbm, rest, sems)
     for copy in copies:
         copy.start()
@@ -163,9 +165,7 @@
         lhs = jnp.concatenate(
             [jnp.where(item == c * CHUNK + i, qc, 0.0) for i in range(CHUNK)], axis=1
         ).astype(jnp.bfloat16)
-        at = c * CHUNK
-        part = kept[pl.ds(at, CHUNK)] if at < KEPT else rest[pl.ds(at - KEPT, CHUNK)]
-        s_high, s_low = halves(part.reshape(CHUNK * DK, DV))
+        s_high, s_low = halves((*kept, *rest)[c][...].reshape(CHUNK * DK, DV))
         num = jnp.dot(lhs, s_high, preferred_element_type=jnp.float32) + jnp.dot(
             lhs, s_low, preferred_element_type=jnp.float32
         )
@@ -184,9 +184,11 @@
 
 
 def memory_kernel(
-    coef_ref, k_ref, ko_ref, values_ref, norm_ref, kept, state_hbm,
-    new_hbm, new_norm_ref, new_max_ref, rest, new, sems, out_sems,
+    coef_ref, k_ref, ko_ref, values_ref, norm_ref, *refs,
 ):
+    kept = refs[: KEPT // CHUNK]
+    state_hbm, new_hbm, new_norm_hbm, new_max_hbm, *rest = refs[KEPT // CHUNK :]
+    *rest, new, new_norm_ref, new_max_ref, sems, out_sems = rest
     copies = state_copies(state_hbm, rest, sems)
     for copy in copies:
         copy.start()
@@ -207,11 +209,18 @@
         + jnp.dot(t_high, kb, preferred_element_type=jnp.float32)
         + jnp.dot(t_low, kb, preferred_element_type=jnp.float32)
     )
+    stores = [
+        pltpu.make_async_copy(src, dst, out_sems.at[CHUNKS + i])
+        for i, (src, dst) in enumerate(
+            ((new_norm_ref, new_norm_hbm), (new_max_ref, new_max_hbm))
+        )
+    ]
+    for store in stores:
+        store.start()
     high, low = halves(k.T * tok)
     both = jnp.concatenate([high, low], axis=1)
     twice = jnp.concatenate([v, v], axis=0)
     lane = item_of(iota((8, 2 * RUN), 1) % RUN)
-    stores = []
     for c in range(CHUNKS):
         if c * CHUNK >= KEPT:
             copies[c - KEPT // CHUNK].wait()
@@ -219,8 +228,7 @@
             mask = (lane == i).astype(jnp.float32)[:1].astype(jnp.bfloat16)
             update = jnp.dot(both * mask, twice, preferred_element_type=jnp.float32)
             at = i // 2 * 8 + i % 2
-            old = kept[i] if i < KEPT else rest[i - KEPT]
-            new[i] = keep[:, at : at + 1] * old + update
+            new[i] = keep[:, at : at + 1] * (*kept, *rest)[c][i - c * CHUNK] + update
         stores.append(
             pltpu.make_async_copy(
                 new.at[pl.ds(c * CHUNK, CHUNK)], new_hbm.at[pl.ds(c * CHUNK, CHUNK)], out_sems.at[c]
@@ -235,10 +243,10 @@
 ANY = pl.BlockSpec(memory_space=pl.ANY)
 
 
-def hidden_of(q, k, ko, v, vo, ig, fg, igo, fgo, accepted, smax, norm, gain, kept, state):
+def hidden_of(q, k, ko, v, vo, ig, fg, igo, fgo, accepted, smax, norm, gain, *kept, state):
     return pl.pallas_call(
         hidden_kernel,
-        in_specs=[VMEM] * 14 + [ANY],
+        in_specs=[VMEM] * (13 + len(kept)) + [ANY],
         out_specs=(VMEM, VMEM, VMEM),
         out_shape=(
             pltpu.VMEM((PROPS, SEQS, HEADS * DV), jnp.bfloat16),
@@ -246,43 +254,53 @@
             pltpu.VMEM((RUN, DV), jnp.bfloat16),
         ),
         scratch_shapes=[
-            pltpu.VMEM((ITEMS - KEPT, DK, DV), jnp.float32),
+            *[pltpu.VMEM((CHUNK, DK, DV), jnp.float32)] * ((ITEMS - KEPT) // CHUNK),
             pltpu.VMEM((2, ROWS, DK), jnp.float32),
             pltpu.SemaphoreType.DMA((CHUNKS,)),
         ],
         name="hidden",
-    )(q, k, ko, v, vo, ig, fg, igo, fgo, accepted, smax, norm, gain, kept, state)
-
-
-def memory_of(coef, k, ko, v, norm, kept, state):
+    )(q, k, ko, v, vo, ig, fg, igo, fgo, accepted, smax, norm, gain, *kept, state)
+
+
+def memory_of(coef, k, ko, v, norm, *kept, state):
     return pl.pallas_call(
         memory_kernel,
-        in_specs=[VMEM] * 6 + [ANY],
-        out_specs=(ANY, VMEM, VMEM),
+        in_specs=[VMEM] * (5 + len(kept)) + [ANY],
+        out_specs=(ANY, ANY, ANY),
         out_shape=(
             jax.ShapeDtypeStruct((ITEMS, DK, DV), jnp.float32),
             jax.ShapeDtypeStruct((ITEMS, DK), jnp.float32),
             jax.ShapeDtypeStruct((HEADS, SEQS), jnp.float32),
         ),
         scratch_shapes=[
-            pltpu.VMEM((ITEMS - KEPT, DK, DV), jnp.float32),
+            *[pltpu.VMEM((CHUNK, DK, DV), jnp.float32)] * ((ITEMS - KEPT) // CHUNK),
             pltpu.VMEM((ITEMS, DK, DV), jnp.float32),
+            pltpu.VMEM((ITEMS, DK), jnp.float32),
+            pltpu.VMEM((HEADS, SEQS), jnp.float32),
             pltpu.SemaphoreType.DMA((CHUNKS,)),
-            pltpu.SemaphoreType.DMA((CHUNKS,)),
+            pltpu.SemaphoreType.DMA((CHUNKS + 2,)),
         ],
         name="memory",
-    )(coef, k, ko, v, norm, kept, state)
+    )(coef, k, ko, v, norm, *kept, state)
 
 
 def front_kernel(block_hbm, *refs):
-    count = (len(refs) - 4) // 2
-    inputs, pieces_hbm, outputs = refs[:count], refs[count], refs[count + 1 : 2 * count + 1]
-    block, pieces, sems = refs[2 * count + 1 :]
+    *refs, block, pieces, sems = refs
+    count = (len(refs) - 2 - KEPT // CHUNK) // 2
+    inputs, state_hbm, pieces_hbm, outputs = (
+        refs[:count], refs[count], refs[count + 1], refs[count + 2 :]
+    )
     first = pltpu.make_async_copy(block_hbm, block, sems.at[0])
     first.start()
     copies = [
-        pltpu.make_async_copy(src.at[pl.ds(0, dst.shape[0])], dst, sems.at[i + 2])
-        for i, (src, dst) in enumerate(zip(inputs, outputs, strict=True))
+        pltpu.make_async_copy(src, dst, sems.at[i + 2])
+        for i, (src, dst) in enumerate(zip(inputs, outputs))
+    ]
+    copies += [
+        pltpu.make_async_copy(
+            state_hbm.at[pl.ds(i * CHUNK, CHUNK)], dst, sems.at[len(inputs) + i + 2]
+        )
+        for i, dst in enumerate(outputs[len(inputs) :])
     ]
     for copy in copies:
         copy.start()
@@ -299,10 +317,10 @@
 def front(block, count, arrays, state):
     shape = (count, *block.shape)
     outs = [pltpu.VMEM(a.shape, a.dtype) for a in arrays]
-    outs.append(pltpu.VMEM((KEPT, *state.shape[1:]), state.dtype))
+    outs += [pltpu.VMEM((CHUNK, *state.shape[1:]), state.dtype)] * (KEPT // CHUNK)
     return pl.pallas_call(
         front_kernel,
-        in_specs=[ANY] * (1 + len(outs)),
+        in_specs=[ANY] * (2 + len(arrays)),
         out_specs=[ANY] + [VMEM] * len(outs),
         out_shape=[jax.ShapeDtypeStruct(shape, block.dtype), *outs],
         scratch_shapes=[
@@ -413,16 +431,17 @@
     inputs = (q, k, ko, v, vo, *gates, accepted[None], state_max.T, norm, norm_gain)
     pieces, *inputs = front(out_weight.T, zs, inputs, state)
     inputs = [in_vmem(a) for a in inputs]
-    q, k, ko, *_, norm, _, kept = inputs
+    q, k, ko = inputs[:3]
+    norm, kept = inputs[11], inputs[13:]
     weight = exchanged(pieces, "kv_0", from_place(FIRST_Z, zs))
     weight = weight.reshape(-1, out_weight.shape[0])
-    hidden, coef, run_values = hidden_of(*inputs, state)
+    hidden, coef, run_values = hidden_of(*inputs, state=state)
     rows = lax.all_gather(hidden.reshape(PROPS * SEQS, -1), PLANE, tiled=True)
     order = [g * tps + t for g in from_place(FIRST_CROSS, cross) for t in from_place(FIRST_TP, tps)]
     terms = product(in_vmem(rows), in_vmem(weight), order)
     terms = exchanged(terms, (*PLANE, "tp"), order)
     new_mem, new_norm, new_max = memory_of(
-        in_vmem(coef), k, ko, in_vmem(run_values), norm, kept, state
+        in_vmem(coef), k, ko, in_vmem(run_values), norm, *kept, state=state
     )
     mixed = joined(in_vmem(terms), order, tps, out_weight.shape[1])[:, None]
     return (

time: 51.5 us -> 49.6 us (0.963)
  Pallas kernels: 9.11 us -> 6.65 us
  local copies, waits for them, and re-layouts: 0 us -> 1.04 us
  starting transfers between devices: 27.3 us -> 26.5 us
    pallas_call x3, Pallas kernels: 7.35 us -> 4.89 us  [the longest x1 1.94 us: front(): pl.pallas_call(front_kernel, in_specs=[ANY] * (2 + len(arrays)), out_spec...]
    unnamed x0 -> x4, local copies, waits for them, and re-layouts: none -> 1.04 us
    all_to_all x2, starting transfers between devices: 27.3 us -> 26.5 us  [exchanged(): lax.all_to_all(pieces, axes, split_axis=0, concat_axis=0, tiled=True, axi...]
  transfers between devices with their start and end apart: 2 -> 2, of which waited for: 0 -> 1; matrix products, arithmetic and copies ran while one was open for 0% -> 0% of each run, Pallas kernels for 11% -> 6%
where the time goes in v5:
time: 49.6 us; the launch traced here: 49.2 us
  starting transfers between devices  26.5 us (53%)
  blocking collectives  14.3 us (29%)
  Pallas kernels  6.65 us (13%)
  local copies, waits for them, and re-layouts  1.04 us (2%)
  between operations  0.7 us (1%)
    all_to_all x2, starting transfers between devices, exchanged(): lax.all_to_all(pieces, axes, split_axis=0, concat_axis=0, tiled=True, axi...  26.5 us
    all_gather x1, blocking collectives, on_device(): rows = lax.all_gather(hidden.reshape(PROPS * SEQS, -1), PLANE, tiled=True)  14.3 us
    pallas_call x1, Pallas kernels, front(): pl.pallas_call(front_kernel, in_specs=[ANY] * (2 + len(arrays)), out_spec...  1.94 us
    pallas_call x1, Pallas kernels, memory_of(): pl.pallas_call(memory_kernel, in_specs=[VMEM] * (5 + len(kept)) + [ANY],...  1.71 us
    pallas_call x1, Pallas kernels, hidden_of(): pl.pallas_call(hidden_kernel, in_specs=[VMEM] * (13 + len(kept)) + [ANY],...  1.23 us
    unnamed x4, local copies, waits for them, and re-layouts  1.04 us
  transfers between devices with their start and end apart: 2, of which 1 were waited for; matrix products, arithmetic and copies ran while one was open for 0% of the time, Pallas kernels for 6%

profile of v5, /device:TPU:1, one launch (start us, length us, event | category | flops | bytes accessed | tf_op | source)
XLA Modules:
  0.0 49.2 jit_solution(2657927913569954285)
XLA Ops:
  0.6 1.9 %front.1 = (bf16[16,16,512]{2,1,0:T(8,128)(2,1)}, bf16[64,128]{1,0:T(8,128)(2,1)S(1)}, bf16[64,128]{1,0:T(8,128)(2,1)S(1)}, bf16[64,128]{1,0:T(8,128)(2,1)S(1)},...) custom-call(bf16[16,512]{1,0:T(8,128)(2,1)} %bitcast.36, ...), custom_call_target="tpu_custom_call" | custom-call | tf_op jit(solution)/shard_map/front/pallas_call | solution.py:321
  2.6 0.0 copy-start
  2.6 15.9 %all-to-all-start = ((bf16[16,16,512]{2,1,0:T(8,128)(2,1)}), bf16[16,16,512]{2,1,0:T(8,128)(2,1)S(1)}, u32[]{:S(2)}, u32[]{:S(2)}) async-start(bf16[16,16,512]{2,1,0:T(8,128)(2,1)} %get-tuple-element.46), calls=%async_computation | async-start | bytes 524288 | tf_op jit(solution)/shard_map/all_to_all | solution.py:390
  18.5 1.2 %hidden.1 = (bf16[4,8,512]{2,1,0:T(8,128)(2,1)S(1)}, f32[8,128]{1,0:T(8,128)S(1)}, bf16[128,256]{1,0:T(8,128)(2,1)S(1)}) custom-call(bf16[64,128]{1,0:T(8,128)(2,1)S(1)} %get-tuple-element.28.q_ref, bf16[64,128]{1,0:T(8,128)(2,1)S(1)} %get-tuple-element.29.k_ref, bf16[64,128]{1,0:T(8,128)(2,1)S(1)} %get-tuple-element.30.ko_ref, ...), custom_call_target="tpu_custom_call" | custom-call | tf_op jit(solution)/shard_map/hidden/pallas_call | solution.py:247
  19.8 0.0 copy-done
  19.8 14.3 %all_gather.3.rows_ref = bf16[256,512]{1,0:T(8,128)(2,1)S(1)} all-gather(bf16[32,512]{1,0:T(8,128)(2,1)S(1)} %bitcast.29), channel_id=1, replica_groups=mesh['kv_0'=16,'kv_1'=4,'kv_2'=2,'tp'=4] {'kv_1','kv_2'}, dimensions={0}, use_global_device_ids=true | all-gather | bytes 294912 | tf_op jit(solution)/shard_map/all_gather | solution.py:439
  34.0 0.0 all-to-all-done
  34.0 0.9 %product.1 = bf16[32,8,256]{2,1,0:T(8,128)(2,1)} custom-call(bf16[256,512]{1,0:T(8,128)(2,1)S(1)} %all_gather.3.rows_ref, bf16[256,512]{1,0:T(8,128)(2,1)S(1)} %bitcast.28), custom_call_target="tpu_custom_call" | custom-call | tf_op jit(solution)/shard_map/product/pallas_call | solution.py:342
  35.0 10.5 %all-to-all-start.1 = ((bf16[32,8,256]{2,1,0:T(8,128)(2,1)}), bf16[32,8,256]{2,1,0:T(8,128)(2,1)S(1)}, u32[]{:S(2)}, u32[]{:S(2)}) async-start(bf16[32,8,256]{2,1,0:T(8,128)(2,1)} %product.1), calls=%async_computation.1 | async-start | bytes 262144 | tf_op jit(solution)/shard_map/all_to_all | solution.py:390
  45.5 0.0 copy-start.1
  45.5 1.0 %copy-done.1 = f32[4,128,256]{2,1,0:T(8,128)S(1)} copy-done((f32[4,128,256]{2,1,0:T(8,128)S(1)}, f32[4,128,256]{2,1,0:T(8,128)}, u32[]{:S(2)}) %copy-start.1) | copy-done | bytes 524312
  46.5 1.7 %memory.1 = (f32[16,128,256]{2,1,0:T(8,128)}, f32[16,128]{1,0:T(8,128)}, f32[2,8]{1,0:T(2,128)}) custom-call(f32[8,128]{1,0:T(8,128)S(1)} %get-tuple-element.47.coef_ref, bf16[64,128]{1,0:T(8,128)(2,1)S(1)} %get-tuple-element.29.k_ref, bf16[64,128]{1,0:T(8,128)(2,1)S(1)} %get-tuple-element.30.ko_ref, bf16[128,256]{1,0:T(8,128)(2,1)S(1)} %get-tuple-element.48.values_ref, ...), custom_call_target="tpu_custom_call" | custom-call | tf_op jit(solution)/shard_map/memory/pallas_call | solution.py:266
  48.3 0.1 all-to-all-done.1.terms_ref
  48.3 0.8 %join.1 = bf16[8,2048]{1,0:T(8,128)(2,1)} custom-call(bf16[32,8,256]{2,1,0:T(8,128)(2,1)S(1)} %all-to-all-done.1.terms_ref), custom_call_target="tpu_custom_call" | custom-call | tf_op jit(solution)/shard_map/join/pallas_call | solution.py:380
Async XLA Ops:
  2.6 17.2 %copy-start = (f32[4,128,256]{2,1,0:T(8,128)}, f32[4,128,256]{2,1,0:T(8,128)S(1)}, u32[]{:S(2)}) copy-start(f32[4,128,256]{2,1,0:T(8,128)S(1)} %get-tuple-element.43.refs_2_) | copy-start | bytes 1572868
  2.6 31.4 %all-to-all-start = ((bf16[16,16,512]{2,1,0:T(8,128)(2,1)}), bf16[16,16,512]{2,1,0:T(8,128)(2,1)S(1)}, u32[]{:S(2)}, u32[]{:S(2)}) async-start(bf16[16,16,512]{2,1,0:T(8,128)(2,1)} %get-tuple-element.46), calls=%async_computation | async-start | bytes 524288 | tf_op jit(solution)/shard_map/all_to_all | solution.py:390
  35.0 13.4 %all-to-all-start.1 = ((bf16[32,8,256]{2,1,0:T(8,128)(2,1)}), bf16[32,8,256]{2,1,0:T(8,128)(2,1)S(1)}, u32[]{:S(2)}, u32[]{:S(2)}) async-start(bf16[32,8,256]{2,1,0:T(8,128)(2,1)} %product.1), calls=%async_computation.1 | async-start | bytes 262144 | tf_op jit(solution)/shard_map/all_to_all | solution.py:390
  45.5 1.0 %copy-start.1 = (f32[4,128,256]{2,1,0:T(8,128)S(1)}, f32[4,128,256]{2,1,0:T(8,128)}, u32[]{:S(2)}) copy-start(f32[4,128,256]{2,1,0:T(8,128)} %copy-done) | copy-start | bytes 1572868

commit v6 on v5

--- a/solution.py
+++ b/solution.py
@@ -23,7 +23,8 @@
 CHUNKS = ITEMS // CHUNK
 KEPT = 16
 EPS = 1e-5
-FIRST_Z, FIRST_CROSS, FIRST_TP = 12, 5, 2
+Z_ORDER = (12, 0, 15, 1, 14, 2, 13, 3, 4, 5, 6, 7, 8, 9, 10, 11)
+FIRST_CROSS, FIRST_TP = 5, 2
 
 
 def iota(shape, dim):
@@ -351,7 +352,6 @@
 def join_kernel(terms_ref, out_ref, *, order, tps, block):
     cross = len(order) // tps
     slot = {source: i for i, source in enumerate(order)}
-    planes = out_ref.shape[1] // DK
     lane = iota((SEQS, DK), 1) // block
     for part in range(terms_ref.shape[2] // DK):
         cols = slice(part * DK, (part + 1) * DK)
@@ -371,7 +371,7 @@
             sums = swapped
             step *= 2
         for z in range(cross):
-            at = (FIRST_Z + part * cross + z) % planes * DK
+            at = Z_ORDER[part * cross + z] * DK
             out_ref[:, at : at + DK] = sums[z].astype(jnp.bfloat16)
 
 
@@ -433,7 +433,7 @@
     inputs = [in_vmem(a) for a in inputs]
     q, k, ko = inputs[:3]
     norm, kept = inputs[11], inputs[13:]
-    weight = exchanged(pieces, "kv_0", from_place(FIRST_Z, zs))
+    weight = exchanged(pieces, "kv_0", list(Z_ORDER))
     weight = weight.reshape(-1, out_weight.shape[0])
     hidden, coef, run_values = hidden_of(*inputs, state=state)
     rows = lax.all_gather(hidden.reshape(PROPS * SEQS, -1), PLANE, tiled=True)

time: 49.6 us -> 48.9 us (0.986)
  starting transfers between devices: 26.5 us -> 25.8 us
    all_to_all x2, starting transfers between devices: 26.5 us -> 25.8 us  [exchanged(): lax.all_to_all(pieces, axes, split_axis=0, concat_axis=0, tiled=True, axi...]
where the time goes in v6:
time: 48.9 us; the launch traced here: 48.5 us
  starting transfers between devices  25.8 us (53%)
  blocking collectives  14.3 us (29%)
  Pallas kernels  6.65 us (14%)
  local copies, waits for them, and re-layouts  1.04 us (2%)
  between operations  0.7 us (1%)
    all_to_all x2, starting transfers between devices, exchanged(): lax.all_to_all(pieces, axes, split_axis=0, concat_axis=0, tiled=True, axi...  25.8 us
    all_gather x1, blocking collectives, on_device(): rows = lax.all_gather(hidden.reshape(PROPS * SEQS, -1), PLANE, tiled=True)  14.3 us
    pallas_call x1, Pallas kernels, front(): pl.pallas_call(front_kernel, in_specs=[ANY] * (2 + len(arrays)), out_spec...  1.94 us
    pallas_call x1, Pallas kernels, memory_of(): pl.pallas_call(memory_kernel, in_specs=[VMEM] * (5 + len(kept)) + [ANY],...  1.72 us
    pallas_call x1, Pallas kernels, hidden_of(): pl.pallas_call(hidden_kernel, in_specs=[VMEM] * (13 + len(kept)) + [ANY],...  1.23 us
    unnamed x4, local copies, waits for them, and re-layouts  1.04 us
  transfers between devices with their start and end apart: 2, of which 1 were waited for; matrix products, arithmetic and copies ran while one was open for 0% of the time, Pallas kernels for 6%

profile of v6, /device:TPU:1, one launch (start us, length us, event | category | flops | bytes accessed | tf_op | source)
XLA Modules:
  0.0 48.5 jit_solution(3430870339199586669)
XLA Ops:
  0.6 1.9 %front.1 = (bf16[16,16,512]{2,1,0:T(8,128)(2,1)}, bf16[64,128]{1,0:T(8,128)(2,1)S(1)}, bf16[64,128]{1,0:T(8,128)(2,1)S(1)}, bf16[64,128]{1,0:T(8,128)(2,1)S(1)},...) custom-call(bf16[16,512]{1,0:T(8,128)(2,1)} %bitcast.36, ...), custom_call_target="tpu_custom_call" | custom-call | tf_op jit(solution)/shard_map/front/pallas_call | solution.py:322
  2.6 0.0 copy-start
  2.6 15.9 %all-to-all-start = ((bf16[16,16,512]{2,1,0:T(8,128)(2,1)}), bf16[16,16,512]{2,1,0:T(8,128)(2,1)S(1)}, u32[]{:S(2)}, u32[]{:S(2)}) async-start(bf16[16,16,512]{2,1,0:T(8,128)(2,1)} %get-tuple-element.46), calls=%async_computation | async-start | bytes 524288 | tf_op jit(solution)/shard_map/all_to_all | solution.py:390
  18.5 1.2 %hidden.1 = (bf16[4,8,512]{2,1,0:T(8,128)(2,1)S(1)}, f32[8,128]{1,0:T(8,128)S(1)}, bf16[128,256]{1,0:T(8,128)(2,1)S(1)}) custom-call(bf16[64,128]{1,0:T(8,128)(2,1)S(1)} %get-tuple-element.28.q_ref, bf16[64,128]{1,0:T(8,128)(2,1)S(1)} %get-tuple-element.29.k_ref, bf16[64,128]{1,0:T(8,128)(2,1)S(1)} %get-tuple-element.30.ko_ref, ...), custom_call_target="tpu_custom_call" | custom-call | tf_op jit(solution)/shard_map/hidden/pallas_call | solution.py:248
  19.8 0.0 copy-done
  19.8 14.3 %all_gather.3.rows_ref = bf16[256,512]{1,0:T(8,128)(2,1)S(1)} all-gather(bf16[32,512]{1,0:T(8,128)(2,1)S(1)} %bitcast.29), channel_id=1, replica_groups=mesh['kv_0'=16,'kv_1'=4,'kv_2'=2,'tp'=4] {'kv_1','kv_2'}, dimensions={0}, use_global_device_ids=true | all-gather | bytes 294912 | tf_op jit(solution)/shard_map/all_gather | solution.py:439
  34.0 0.0 all-to-all-done
  34.0 0.9 %product.1 = bf16[32,8,256]{2,1,0:T(8,128)(2,1)} custom-call(bf16[256,512]{1,0:T(8,128)(2,1)S(1)} %all_gather.3.rows_ref, bf16[256,512]{1,0:T(8,128)(2,1)S(1)} %bitcast.28), custom_call_target="tpu_custom_call" | custom-call | tf_op jit(solution)/shard_map/product/pallas_call | solution.py:343
  35.0 9.8 %all-to-all-start.1 = ((bf16[32,8,256]{2,1,0:T(8,128)(2,1)}), bf16[32,8,256]{2,1,0:T(8,128)(2,1)S(1)}, u32[]{:S(2)}, u32[]{:S(2)}) async-start(bf16[32,8,256]{2,1,0:T(8,128)(2,1)} %product.1), calls=%async_computation.1 | async-start | bytes 262144 | tf_op jit(solution)/shard_map/all_to_all | solution.py:390
  44.8 0.0 copy-start.1
  44.8 1.0 %copy-done.1 = f32[4,128,256]{2,1,0:T(8,128)S(1)} copy-done((f32[4,128,256]{2,1,0:T(8,128)S(1)}, f32[4,128,256]{2,1,0:T(8,128)}, u32[]{:S(2)}) %copy-start.1) | copy-done | bytes 524312
  45.8 1.7 %memory.1 = (f32[16,128,256]{2,1,0:T(8,128)}, f32[16,128]{1,0:T(8,128)}, f32[2,8]{1,0:T(2,128)}) custom-call(f32[8,128]{1,0:T(8,128)S(1)} %get-tuple-element.47.coef_ref, bf16[64,128]{1,0:T(8,128)(2,1)S(1)} %get-tuple-element.29.k_ref, bf16[64,128]{1,0:T(8,128)(2,1)S(1)} %get-tuple-element.30.ko_ref, bf16[128,256]{1,0:T(8,128)(2,1)S(1)} %get-tuple-element.48.values_ref, ...), custom_call_target="tpu_custom_call" | custom-call | tf_op jit(solution)/shard_map/memory/pallas_call | solution.py:267
  47.6 0.1 all-to-all-done.1.terms_ref
  47.6 0.8 %join.1 = bf16[8,2048]{1,0:T(8,128)(2,1)} custom-call(bf16[32,8,256]{2,1,0:T(8,128)(2,1)S(1)} %all-to-all-done.1.terms_ref), custom_call_target="tpu_custom_call" | custom-call | tf_op jit(solution)/shard_map/join/pallas_call | solution.py:380
Async XLA Ops:
  2.6 17.2 %copy-start = (f32[4,128,256]{2,1,0:T(8,128)}, f32[4,128,256]{2,1,0:T(8,128)S(1)}, u32[]{:S(2)}) copy-start(f32[4,128,256]{2,1,0:T(8,128)S(1)} %get-tuple-element.43.refs_2_) | copy-start | bytes 1572868
  2.6 31.4 %all-to-all-start = ((bf16[16,16,512]{2,1,0:T(8,128)(2,1)}), bf16[16,16,512]{2,1,0:T(8,128)(2,1)S(1)}, u32[]{:S(2)}, u32[]{:S(2)}) async-start(bf16[16,16,512]{2,1,0:T(8,128)(2,1)} %get-tuple-element.46), calls=%async_computation | async-start | bytes 524288 | tf_op jit(solution)/shard_map/all_to_all | solution.py:390
  35.0 12.7 %all-to-all-start.1 = ((bf16[32,8,256]{2,1,0:T(8,128)(2,1)}), bf16[32,8,256]{2,1,0:T(8,128)(2,1)S(1)}, u32[]{:S(2)}, u32[]{:S(2)}) async-start(bf16[32,8,256]{2,1,0:T(8,128)(2,1)} %product.1), calls=%async_computation.1 | async-start | bytes 262144 | tf_op jit(solution)/shard_map/all_to_all | solution.py:390
  44.8 1.0 %copy-start.1 = (f32[4,128,256]{2,1,0:T(8,128)S(1)}, f32[4,128,256]{2,1,0:T(8,128)}, u32[]{:S(2)}) copy-start(f32[4,128,256]{2,1,0:T(8,128)} %copy-done) | copy-start | bytes 1572868
